TPU v7x, 32 devices: a whole 2x2x4 slice. The times are simulated.
32 devices in a mesh: sp: 4 (over y, x), tp: 8 (over z, core).
Axes of the slice: x: 2, y: 2, z: 4, core: 2. Of those that a mesh axis runs over, the one named last changes fastest.
Arguments:
- stream: bfloat16 [4096, 1024], P('tp', 'sp'), may hold values from -6 to 6
- value_weight: bfloat16 [2, 2048, 4096], P(None, 'tp', 'sp'), may hold values from -0.09375 to 0.09375
- gate_weight: bfloat16 [2, 2048, 4096], P(None, 'tp', 'sp'), may hold values from -0.09375 to 0.09375
- conv_taps: bfloat16 [2, 2048, 31], P(None, 'tp'), may hold values from -16 to 16
- norm_gain: bfloat16 [2, 2048], P(None, 'tp'), may hold values from 0.099609375 to 1.8984375
- out_weight: bfloat16 [2, 4096, 2048], P(None, 'tp', 'sp'), may hold values from -4 to 4
- out_gain: bfloat16 [2, 4096], P(None, 'tp'), may hold values from 0.099609375 to 1.8984375
Outputs:
- result: bfloat16 [4096, 1024], P('tp', 'sp')
All inputs are finite; a program needn't handle non-finite values.
Results may differ from a plain program's by a relative error of at most 0.015.
Values may be sent and summed in bfloat16 or wider, within the bound.
A program may use at most 64 MiB of HBM per device.

v0:
```python
import functools

import jax
import jax.numpy as jnp
from jax import lax
from jax.experimental import pallas as pl
from jax.experimental.pallas import tpu as pltpu
from jax.sharding import PartitionSpec as P

MESH = pl.DeviceIdType.MESH
F32 = jnp.float32
BF16 = jnp.bfloat16
LANES = 128
CONV_ROWS = 16


def grid_of(count):
    nx = int(count**0.5)
    while count % nx:
        nx -= 1
    return count // nx, nx


def kernel(
    n_sp, n_tp, n_layers,
    stream, value_w, gate_w, taps, norm_gain, out_w, out_gain,
    result,
    h_all, conv_all, branch_all, active, v_buf, g_buf, o_buf, gat, halo_l, halo_r, acc, sums, squares,
    norm_rows, out_rows, norm_cols, out_cols,
    local_sem, send_sem, recv_sem,
):
    ny, nx = grid_of(n_sp)
    nz = n_tp // 2
    s, t = lax.axis_index("sp"), lax.axis_index("tp")
    y, x = s // nx, s % nx
    z, c = t // 2, t % 2
    features, positions = stream.shape
    channels = value_w.shape[1]
    f_cols = value_w.shape[2]
    c_cols = out_w.shape[2]
    width = channels * n_tp
    model = features * n_tp
    n_taps = taps.shape[2]
    reach = n_taps // 2
    counter = [0]
    sent = []

    def remote(src, dst, sp, tp):
        i = counter[0]
        counter[0] += 1
        return pltpu.make_async_remote_copy(
            src_ref=src, dst_ref=dst, send_sem=send_sem.at[i], recv_sem=recv_sem.at[i],
            device_id={"sp": sp, "tp": tp}, device_id_type=MESH,
        )

    def start(copy, condition=None):
        if condition is None:
            copy.start()
        else:
            pl.when(condition)(copy.start)
        sent.append((copy, condition))

    def slot_of(k, j):
        return lax.rem(y + ny - k, ny) * nx + lax.rem(x + nx - j, nx)

    def x_peer(j):
        return y * nx + lax.rem(x + j, nx)

    def y_peer(k):
        return lax.rem(y + k, ny) * nx + x

    class Gather:
        def __init__(self, src, dst, x_first):
            self.copies = {}
            self.x_first = x_first
            for k in range(ny):
                for j in range(nx):
                    if k == 0 and j == 0:
                        continue
                    if x_first:
                        along_x = k == 0
                        origin = (0, 0) if along_x else (0, j)
                    else:
                        along_x = j > 0
                        origin = (k, 0) if along_x else (0, 0)
                    own = origin == (0, 0)
                    target = x_peer(j) if along_x else y_peer(k)
                    origin_slot = slot_of(*origin)
                    self.copies[k, j] = (
                        remote(src if own else dst(origin_slot), dst(origin_slot), target, t),
                        own, origin,
                    )
            i = local_count[0]
            local_count[0] += 1
            self.local = pltpu.make_async_copy(src, dst(s), local_sem.at[i])
            self.here = set()

        def start_own(self, first):
            for (k, j), (copy, own, _) in self.copies.items():
                if own and first == ((k == 0) == self.x_first):
                    start(copy)
            if first:
                self.local.start()

        def forward(self):
            for copy, own, origin in self.copies.values():
                if not own:
                    self.arrive(*origin)
                    start(copy)

        def arrive(self, k, j):
            if (k, j) not in self.here:
                self.here.add((k, j))
                if k == 0 and j == 0:
                    self.local.wait()
                else:
                    self.copies[k, j][0].wait_recv()

    local_count = [0]

    def start_pair(pair):
        for first in (True, False):
            for gather in pair:
                gather.start_own(first)

    def forward_pair(pair):
        for gather in pair:
            gather.forward()

    class Spread:
        def __init__(self, buf, rows, src):
            def place(zz, cc):
                row = pl.multiple_of((jnp.clip(zz, 0, nz - 1) * 2 + cc) * rows, rows)
                return buf.at[pl.ds(row, rows), :]

            self.across = remote(src, place(z, c), s, z * 2 + 1 - c)
            self.along, self.hand, self.has = {}, {}, {}
            for way in (1, -1):
                after = jnp.clip(z + way, 0, nz - 1) * 2 + c
                for d in range(1, nz):
                    carried = z - way * (d - 1)
                    origin = src if d == 1 else place(carried, c)
                    self.along[way, d] = remote(origin, place(carried, c), s, after)
                    self.has[way, d] = (z - way * d >= 0) & (z - way * d < nz)
                    seen = place(z - way * d, c)
                    self.hand[way, d] = remote(seen, seen, s, z * 2 + 1 - c)

        def send(self, way, d):
            holds = (z - way * (d - 1) >= 0) & (z - way * (d - 1) < nz)
            more = (z + way >= 0) & (z + way < nz)
            start(self.along[way, d], holds & more)

        def start_own(self):
            for way in (1, -1):
                self.send(way, 1)
            start(self.across)

        def step(self, d):
            for way in (1, -1):
                pl.when(self.has[way, d])(self.along[way, d].wait_recv)
                if d + 1 < nz:
                    self.send(way, d + 1)
                start(self.hand[way, d], self.has[way, d])

        def finish(self):
            self.across.wait_recv()
            for (way, d), hand in self.hand.items():
                pl.when(self.has[way, d])(hand.wait_recv)

    def exchange(src, buf):
        copies = []
        for k in range(1, n_tp):
            copies.append(remote(src, buf.at[t], s, lax.rem(t + k, n_tp)))
            start(copies[-1])
        return copies

    def arrived(copies):
        for copy in copies:
            copy.wait_recv()

    def drain(spread, consume, between):
        consume(t)
        spread.across.wait_recv()
        consume(z * 2 + 1 - c)
        for d in range(1, nz):
            spread.step(d)
            if d == 1:
                between()
            for way in (1, -1):
                @pl.when(spread.has[way, d])
                def _():
                    consume((z - way * d) * 2 + c)
            for way in (1, -1):
                @pl.when(spread.has[way, d])
                def _():
                    spread.hand[way, d].wait_recv()
                    consume((z - way * d) * 2 + 1 - c)

    barrier = pltpu.get_barrier_semaphore()
    for k in range(1, n_sp):
        pl.semaphore_signal(
            barrier, inc=1, device_id={"sp": lax.rem(s + k, n_sp), "tp": t}, device_id_type=MESH
        )
    for k in range(1, n_tp):
        pl.semaphore_signal(
            barrier, inc=1, device_id={"sp": s, "tp": lax.rem(t + k, n_tp)}, device_id_type=MESH
        )
    pl.semaphore_wait(barrier, n_sp + n_tp - 2)

    half = features // 2
    in_proj, out_proj = [], []
    for l in range(n_layers):
        in_proj.append((
            Gather(value_w.at[l], lambda q, l=l: v_buf.at[l, q], True),
            Gather(gate_w.at[l], lambda q, l=l: g_buf.at[l, q], False),
        ))
        out_proj.append((
            Gather(out_w.at[l, pl.ds(0, half)], lambda q, l=l: o_buf.at[l, q, pl.ds(0, half)], True),
            Gather(
                out_w.at[l, pl.ds(half, half)], lambda q, l=l: o_buf.at[l, q, pl.ds(half, half)], False
            ),
        ))

    my_rows = pl.ds(pl.multiple_of(t * features, features), features)
    my_channels = pl.ds(pl.multiple_of(t * channels, channels), channels)
    stream_copy = pltpu.make_async_copy(stream, h_all.at[0, my_rows, :], local_sem.at[4 * n_layers])
    stream_copy.start()
    spread = Spread(h_all.at[0], features, stream)
    spread.start_own()
    start_pair(in_proj[0])
    norm_rows[t] = norm_gain[...]
    out_rows[t] = out_gain[...]
    gain_copies = exchange(norm_gain, norm_rows) + exchange(out_gain, out_rows)

    def to_columns(rows_ref, cols_ref, count):
        def turn(i, carry):
            rows = rows_ref[i].astype(F32)
            fill = jnp.zeros((8 - n_layers, count), F32)
            place = pl.ds(pl.multiple_of(i * count, count), count)
            cols_ref[place, :] = jnp.concatenate([rows, fill], axis=0).T
            return carry

        lax.fori_loop(0, n_tp, turn, 0)

    steps = [(k, j) for k in range(ny) for j in range(nx)]
    right, left = lax.rem(s + 1, n_sp), lax.rem(s + n_sp - 1, n_sp)

    for l in range(n_layers):
        if l == 0:
            for d in range(1, nz):
                if d == nz - 1:
                    forward_pair(in_proj[0])
                spread.step(d)
            spread.finish()
            stream_copy.wait()
            arrived(gain_copies)
            to_columns(norm_rows, norm_cols, channels)
            to_columns(out_rows, out_cols, features)
        for k, j in steps:
            slot = slot_of(k, j)
            rows = pl.ds(pl.multiple_of(slot * f_cols, f_cols), f_cols)
            for half_index, (gather, buf) in enumerate(zip(in_proj[l], (v_buf, g_buf))):
                gather.arrive(k, j)
                part = jnp.dot(buf[l, slot], h_all[l, rows, :], preferred_element_type=F32)
                if (k, j) == (0, 0):
                    acc[half_index] = part
                else:
                    acc[half_index] += part
        gat[l] = (acc[0] * jax.nn.sigmoid(acc[1])).astype(BF16)

        to_right = remote(gat.at[l, :, pl.ds(positions - LANES, LANES)], halo_l.at[l], right, t)
        to_left = remote(gat.at[l, :, pl.ds(0, LANES)], halo_r.at[l], left, t)

        @pl.when(s < n_sp - 1)
        def _():
            to_right.start()

        @pl.when(s > 0)
        def _():
            to_left.start()

        start_pair(out_proj[l])

        @pl.when(s == 0)
        def _():
            halo_l[l] = jnp.zeros_like(halo_l[l])

        @pl.when(s == n_sp - 1)
        def _():
            halo_r[l] = jnp.zeros_like(halo_r[l])

        @pl.when(s > 0)
        def _():
            to_right.wait_recv()

        @pl.when(s < n_sp - 1)
        def _():
            to_left.wait_recv()

        def conv_step(i, carry):
            rows = pl.ds(pl.multiple_of(i * CONV_ROWS, CONV_ROWS), CONV_ROWS)
            wide = jnp.concatenate(
                [halo_l[l, rows, :].astype(F32), gat[l, rows, :].astype(F32), halo_r[l, rows, :].astype(F32)],
                axis=1,
            )
            extent = wide.shape[1]
            weights = taps[l, rows, :].astype(F32)
            total = jnp.zeros((CONV_ROWS, positions), F32)
            for offset in range(n_taps):
                moved = pltpu.roll(wide, (reach - offset) % extent, 1)
                total = total + weights[:, offset : offset + 1] * moved[:, LANES : LANES + positions]
            narrow = total.astype(BF16)
            conv_all[l, pl.ds(pl.multiple_of(t * channels + i * CONV_ROWS, CONV_ROWS), CONV_ROWS), :] = narrow
            value = narrow.astype(F32)
            return (
                carry[0] + jnp.sum(value, axis=0, keepdims=True),
                carry[1] + jnp.sum(value * value, axis=0, keepdims=True),
            )

        zero = jnp.zeros((1, positions), F32)
        own_sum, own_square = lax.fori_loop(0, channels // CONV_ROWS, conv_step, (zero, zero))
        sums[l, t, 0:1, :] = own_sum
        sums[l, t, 1:2, :] = own_square
        sum_copies = exchange(sums.at[l, t], sums.at[l])
        conv_spread = Spread(conv_all.at[l], channels, conv_all.at[l, my_channels, :])
        conv_spread.start_own()
        forward_pair(out_proj[l])
        if l + 1 < n_layers:
            start_pair(in_proj[l + 1])
        arrived(sum_copies)
        channel_totals = jnp.sum(sums[l], axis=0)
        average = channel_totals[0:1] / width
        variance = channel_totals[1:2] / width - average * average
        inverse = lax.rsqrt(variance + 1e-05)

        def activate(block):
            rows = pl.ds(pl.multiple_of(block * channels, channels), channels)
            gain = norm_cols[rows, l : l + 1]
            scaled = (conv_all[l, rows, :].astype(F32) - average) * inverse * gain
            active[rows, :] = (scaled / (1.0 + jnp.exp(-scaled))).astype(BF16)

        drain(conv_spread, activate, lambda: None)
        total = None
        for k, j in steps:
            slot = slot_of(k, j)
            rows = pl.ds(pl.multiple_of(slot * c_cols, c_cols), c_cols)
            for gather in out_proj[l]:
                gather.arrive(k, j)
            part = jnp.dot(o_buf[l, slot], active[rows, :], preferred_element_type=F32)
            total = part if total is None else total + part
        narrow_branch = total.astype(BF16)
        branch = narrow_branch.astype(F32)
        squares[l, t, 0:1, :] = jnp.sum(branch * branch, axis=0, keepdims=True)
        square_copies = exchange(squares.at[l, t], squares.at[l])
        last = l + 1 == n_layers
        if not last:
            branch_all[l, my_rows, :] = narrow_branch
            spread = Spread(branch_all.at[l], features, branch_all.at[l, my_rows, :])
            spread.start_own()
        arrived(square_copies)
        factor = lax.rsqrt(jnp.sum(squares[l], axis=0) / model + 1e-06)
        if last:
            gain = out_cols[my_rows, l : l + 1]
            fresh = h_all[l, my_rows, :].astype(F32) + branch * factor * gain
            result[...] = fresh.astype(BF16)
        else:

            def renew(block):
                rows = pl.ds(pl.multiple_of(block * features, features), features)
                gain = out_cols[rows, l : l + 1]
                change = branch_all[l, rows, :].astype(F32) * factor * gain
                h_all[l + 1, rows, :] = (h_all[l, rows, :].astype(F32) + change).astype(BF16)

            drain(spread, renew, lambda: forward_pair(in_proj[l + 1]))

        @pl.when(s < n_sp - 1)
        def _():
            to_right.wait_send()

        @pl.when(s > 0)
        def _():
            to_left.wait_send()

    for copy, condition in sent:
        if condition is None:
            copy.wait_send()
        else:
            pl.when(condition)(copy.wait_send)


def on_device(n_sp, n_tp, stream, value_weight, gate_weight, conv_taps, norm_gain, out_weight, out_gain):
    layers, channels, f_cols = value_weight.shape
    features, positions = stream.shape
    c_cols = out_weight.shape[2]
    copies = layers * (4 * (n_sp - 1) + 2 + 2 * (n_tp - 1) + 2 * (4 * (n_tp // 2 - 1) + 1)) + 2 * (n_tp - 1)
    vmem = pl.BlockSpec(memory_space=pltpu.VMEM)
    hbm = pl.BlockSpec(memory_space=pl.ANY)
    return pl.pallas_call(
        functools.partial(kernel, n_sp, n_tp, layers),
        out_shape=jax.ShapeDtypeStruct(stream.shape, BF16),
        in_specs=[hbm, hbm, hbm, vmem, vmem, hbm, vmem],
        out_specs=vmem,
        scratch_shapes=[
            pltpu.VMEM((layers, n_tp * features, positions), BF16),
            pltpu.VMEM((layers, n_tp * channels, positions), BF16),
            pltpu.VMEM((max(layers - 1, 1), n_tp * features, positions), BF16),
            pltpu.VMEM((n_tp * channels, positions), BF16),
            pltpu.VMEM((layers, n_sp, channels, f_cols), BF16),
            pltpu.VMEM((layers, n_sp, channels, f_cols), BF16),
            pltpu.VMEM((layers, n_sp, features, c_cols), BF16),
            pltpu.VMEM((layers, channels, positions), BF16),
            pltpu.VMEM((layers, channels, LANES), BF16),
            pltpu.VMEM((layers, channels, LANES), BF16),
            pltpu.VMEM((2, channels, positions), F32),
            pltpu.VMEM((layers, n_tp, 2, positions), F32),
            pltpu.VMEM((layers, n_tp, 1, positions), F32),
            pltpu.VMEM((n_tp, layers, channels), BF16),
            pltpu.VMEM((n_tp, layers, features), BF16),
            pltpu.VMEM((n_tp * channels, 8), F32),
            pltpu.VMEM((n_tp * features, 8), F32),
            pltpu.SemaphoreType.DMA((4 * layers + 1,)),
            pltpu.SemaphoreType.DMA((copies,)),
            pltpu.SemaphoreType.DMA((copies,)),
        ],
        compiler_params=pltpu.CompilerParams(
            collective_id=0, has_side_effects=True, vmem_limit_bytes=60 * 1024 * 1024
        ),
    )(stream, value_weight, gate_weight, conv_taps, norm_gain, out_weight, out_gain)


def solution(mesh):
    return jax.shard_map(
        functools.partial(on_device, mesh.shape["sp"], mesh.shape["tp"]),
        mesh=mesh,
        in_specs=(
            P("tp", "sp"),
            P(None, "tp", "sp"),
            P(None, "tp", "sp"),
            P(None, "tp", None),
            P(None, "tp"),
            P(None, "tp", "sp"),
            P(None, "tp"),
        ),
        out_specs=P("tp", "sp"),
        check_vma=False,
    )
```

profile of v0, /device:TPU:0, one launch (start us, length us, event | category | flops | bytes accessed | tf_op | source)
XLA Modules:
  0.0 131.2 jit_solution(8446631527920170012)
XLA Ops:
  0.0 1.5 %copy.8.taps = bf16[2,256,31]{2,1,0:T(8,128)(2,1)} copy(bf16[2,256,31]{1,0,2:T(2,128)(2,1)} %param.10) | data formatting | bytes 63488 | tf_op args[3]
  1.5 127.9 %shard_map.73 = bf16[512,256]{1,0:T(8,128)(2,1)} custom-call(bf16[512,256]{1,0:T(8,128)(2,1)} %stream.1, bf16[2,256,1024]{2,1,0:T(8,128)(2,1)} %value_w.1, bf16[2,256,1024]{2,1,0:T(8,128)(2,1)} %gate_w.1, bf16[2,256,31]{2,1,0:T(8,128)(2,1)} %copy.8.taps, bf16[2,256]{1,0:T(2,128)(2,1)} %norm_gain.1, bf16[2,512,512]{2,1,0:T(8,128)(2,1)} %out_w.1, ...), custom_call_target="tpu_custom_call" | custom-call | tf_op jit(solution)/shard_map/pallas_call | solution.py:398
  129.5 1.7 %copy.10 = bf16[512,256]{1,0:T(8,128)(2,1)} copy(bf16[512,256]{1,0:T(8,128)(2,1)} %shard_map.73) | data formatting | bytes 524288
where the time goes:
time: 131 us
  Pallas kernels  128 us (98%)
  local copies, waits for them, and re-layouts  3.21 us (2%)
    pallas_call x1, Pallas kernels, on_device(): pl.pallas_call(functools.partial(kernel, n_sp, n_tp, layers), out_shape=j...  128 us
    unnamed x2, local copies, waits for them, and re-layouts  3.21 us

commit v1 on v0

v1 whole, which is shorter than its diff:
```python
import functools

import jax
import jax.numpy as jnp
from jax import lax
from jax.experimental import pallas as pl
from jax.experimental.pallas import tpu as pltpu
from jax.sharding import PartitionSpec as P

MESH = pl.DeviceIdType.MESH
F32 = jnp.float32
BF16 = jnp.bfloat16
LANES = 128
EDGE = 16
TILE = 64


def grid_of(count):
    nx = int(count**0.5)
    while count % nx:
        nx -= 1
    return count // nx, nx


def pieces_of(rows, size):
    return max(1, rows // size)


def kernel(
    n_sp, n_tp, n_layers,
    stream, value_w, gate_w, taps, norm_gain, out_w, out_gain,
    result,
    h_all, x_all, conv_all, branch_all, active, v_buf, g_buf, o_buf, part_out, part_in, wide, flat, tap_rows,
    acc, sums, squares, norm_rows, out_rows, norm_cols, out_cols,
    local_sem, send_sem, recv_sem,
):
    ny, nx = grid_of(n_sp)
    nz = n_tp // 2
    s, t = lax.axis_index("sp"), lax.axis_index("tp")
    y, x = s // nx, s % nx
    z, c = t // 2, t % 2
    features, positions = stream.shape
    channels = value_w.shape[1]
    f_cols = value_w.shape[2]
    c_cols = out_w.shape[2]
    width = channels * n_tp
    model = features * n_tp
    n_taps = taps.shape[2]
    reach = n_taps // 2
    groups = pieces_of(channels, LANES)
    group = channels // groups
    counter = [0]
    sent = []

    def remote(src, dst, sp, tp, width=1, pick=0):
        i = counter[0]
        counter[0] += width
        return pltpu.make_async_remote_copy(
            src_ref=src, dst_ref=dst, send_sem=send_sem.at[i], recv_sem=recv_sem.at[i + pick],
            device_id={"sp": sp, "tp": tp}, device_id_type=MESH,
        )

    def start(copy, condition=None):
        if condition is None:
            copy.start()
        else:
            pl.when(condition)(copy.start)
        sent.append((copy, condition))

    def slot_of(k, j):
        return lax.rem(y + ny - k, ny) * nx + lax.rem(x + nx - j, nx)

    def x_peer(j):
        return y * nx + lax.rem(x + j, nx)

    def y_peer(k):
        return lax.rem(y + k, ny) * nx + x

    local_count = [0]

    def local_copy(src, dst):
        i = local_count[0]
        local_count[0] += 1
        copy = pltpu.make_async_copy(src, dst, local_sem.at[i])
        copy.start()
        return copy

    class Gather:
        def __init__(self, src, dst, x_first, whole=True):
            self.copies, self.own_x, self.own_y, self.relays = {}, [], [], []
            for k in range(ny):
                for j in range(nx if whole else 1):
                    if k == 0 and j == 0:
                        continue
                    if x_first:
                        along_x = k == 0
                        origin = (0, 0) if along_x else (0, j)
                    else:
                        along_x = j > 0
                        origin = (k, 0) if along_x else (0, 0)
                    own = origin == (0, 0)
                    target = x_peer(j) if along_x else y_peer(k)
                    origin_slot = slot_of(*origin)
                    copy = remote(src if own else dst(origin_slot), dst(origin_slot), target, t)
                    self.copies[k, j] = copy
                    if not own:
                        self.relays.append((copy, origin))
                    elif along_x:
                        self.own_x.append(copy)
                    else:
                        self.own_y.append(copy)
            self.local = local_copy(src, dst(s))
            self.here, self.done = set(), set()

        def once(self, name):
            fresh = name not in self.done
            self.done.add(name)
            return fresh

        def send_x(self):
            if self.once("x"):
                for copy in self.own_x:
                    start(copy)

        def send_y(self):
            if self.once("y"):
                for copy in self.own_y:
                    start(copy)

        def relay(self):
            if self.once("relay"):
                for copy, origin in self.relays:
                    self.arrive(*origin)
                    start(copy)

        def flush(self):
            self.send_x()
            self.send_y()
            self.relay()

        def arrive(self, k, j):
            if (k, j) not in self.here:
                self.here.add((k, j))
                if k == 0 and j == 0:
                    self.local.wait()
                else:
                    self.copies[k, j].wait_recv()

    def gathers(w_ref, buf, l, orders, whole=True):
        rows = w_ref.shape[1] // len(orders)
        made = []
        for i, x_first in enumerate(orders):
            part = pl.ds(i * rows, rows)
            made.append(Gather(w_ref.at[l, part], lambda q, part=part: buf.at[l, q, part], x_first, whole))
        return made

    class Spread:
        def __init__(self, buf, rows, pieces, src):
            size = rows // pieces

            def place(zz, cc, k):
                row = pl.multiple_of((jnp.clip(zz, 0, nz - 1) * 2 + cc) * rows + k * size, size)
                return buf.at[pl.ds(row, size), :]

            self.pieces, self.place, self.src = pieces, place, src
            self.across = [remote(src(k), place(z, c, k), s, z * 2 + 1 - c) for k in range(pieces)]
            self.along, self.hand, self.has = {}, {}, {}
            for way in (1, -1):
                after = jnp.clip(z + way, 0, nz - 1) * 2 + c
                for d in range(1, nz):
                    self.has[way, d] = (z - way * d >= 0) & (z - way * d < nz)
                    for k in range(pieces):
                        carried = z - way * (d - 1)
                        origin = src(k) if d == 1 else place(carried, c, k)
                        self.along[way, d, k] = remote(origin, place(carried, c, k), s, after)
                        seen = place(z - way * d, c, k)
                        self.hand[way, d, k] = remote(seen, seen, s, z * 2 + 1 - c)

        def send(self, way, d, k):
            holds = (z - way * (d - 1) >= 0) & (z - way * (d - 1) < nz)
            more = (z + way >= 0) & (z + way < nz)
            start(self.along[way, d, k], holds & more)

        def start_own(self, k):
            for way in (1, -1):
                self.send(way, 1, k)
            start(self.across[k])

        def step(self, d, k, extra=None):
            for way in (1, -1):
                pl.when(self.has[way, d])(self.along[way, d, k].wait_recv)
                if d + 1 < nz:
                    self.send(way, d + 1, k)
                start(self.hand[way, d, k], self.has[way, d])
                if extra is not None:
                    extra(way, d, k)

        def wait_across(self):
            for copy in self.across:
                copy.wait_recv()

        def wait_hand(self, way, d):
            for k in range(self.pieces):
                self.hand[way, d, k].wait_recv()

    class Cross:
        def __init__(self, spread):
            self.spread = spread
            self.size = features // spread.pieces
            self.base, self.hands = {}, {}

        def facts(self, way, d):
            zz = z - way * d
            ok = (zz >= 0) & (zz < nz)
            q = jnp.clip(zz, 0, nz - 1)
            return ok, q, lax.rem(q, nx)

        def rows(self, q, k):
            row = (q // nx * 2 + c) * features + k * self.size
            return pl.ds(pl.multiple_of(row, self.size), self.size)

        def forward(self, way, d, k):
            ok, q, owner = self.facts(way, d)
            pick = jnp.clip(lax.rem(owner - x + nx, nx) - 1, 0, nx - 2)
            self.base[way, d, k] = counter[0]
            src = self.spread.src(k) if d == 0 else self.spread.place(q, c, k)
            copy = remote(
                src, x_all.at[pick, self.rows(q, k), :], y * nx + owner, t, width=nx - 1, pick=pick
            )
            start(copy, ok & (owner != x))

        def receive(self, way, d, k):
            ok, q, owner = self.facts(way, d)
            mine = ok & (owner == x)
            base = self.base[way, d, k]
            for j in range(1, nx):
                here = x_all.at[j - 1, self.rows(q, k), :]
                landed = pltpu.make_async_remote_copy(
                    src_ref=here, dst_ref=here, send_sem=send_sem.at[base], recv_sem=recv_sem.at[base + j - 1],
                    device_id={"sp": s, "tp": z * 2 + 1 - c}, device_id_type=MESH,
                )
                pl.when(mine)(landed.wait_recv)
                hand = remote(here, here, s, z * 2 + 1 - c)
                start(hand, mine)
                self.hands[way, d, k, j] = (hand, mine)

        def finish(self):
            for hand, mine in self.hands.values():
                pl.when(mine)(hand.wait_recv)

    def exchange(src, buf):
        copies = []
        for k in range(1, n_tp):
            copies.append(remote(src, buf.at[t], s, lax.rem(t + k, n_tp)))
            start(copies[-1])
        return copies

    def arrived(copies):
        for copy in copies:
            copy.wait_recv()

    my_rows = pl.ds(pl.multiple_of(t * features, features), features)
    my_channels = pl.ds(pl.multiple_of(t * channels, channels), channels)
    stream_pieces = pieces_of(features, 128)
    conv_pieces = groups * pieces_of(group, 64)

    def rows_of(ref, rows, pieces):
        size = rows // pieces
        return lambda k: ref.at[pl.ds(k * size, size), :]

    stream_copy = local_copy(stream, h_all.at[0, my_rows, :])
    barrier = pltpu.get_barrier_semaphore()
    for k in range(1, n_sp):
        pl.semaphore_signal(
            barrier, inc=1, device_id={"sp": lax.rem(s + k, n_sp), "tp": t}, device_id_type=MESH
        )
    for k in range(1, n_tp):
        pl.semaphore_signal(
            barrier, inc=1, device_id={"sp": s, "tp": lax.rem(t + k, n_tp)}, device_id_type=MESH
        )
    in_proj, out_proj = [], []
    out_parts = pieces_of(features, 128)
    for l in range(n_layers):
        if l == 0:
            v_parts = gathers(value_w, v_buf, l, [True], whole=False)
            g_parts = gathers(gate_w, g_buf, l, [True], whole=False)
        else:
            v_parts = gathers(value_w, v_buf, l, [True, True])
            g_parts = gathers(gate_w, g_buf, l, [False, False])
        in_proj.append((v_parts, g_parts))
        last = l + 1 == n_layers
        out_proj.append(gathers(out_w, o_buf, l, [last] * out_parts))
    norm_rows[t] = norm_gain[...]
    out_rows[t] = out_gain[...]
    for l in range(n_layers):
        padded = jnp.concatenate([taps[l].astype(F32), jnp.zeros((channels, LANES - n_taps), F32)], axis=1)
        tap_rows[l] = padded.T[: 2 * EDGE]
    stream_copy.wait()
    pl.semaphore_wait(barrier, n_sp + n_tp - 2)

    spread = Spread(
        h_all.at[0], features, stream_pieces, rows_of(h_all.at[0, my_rows, :], features, stream_pieces)
    )
    cross = Cross(spread)
    for k in range(stream_pieces):
        spread.start_own(k)
        cross.forward(1, 0, k)
    for part in in_proj[0][0] + in_proj[0][1]:
        part.send_y()
    out_proj[0][0].send_x()
    gain_copies = exchange(norm_gain, norm_rows) + exchange(out_gain, out_rows)

    def to_columns(rows_ref, cols_ref, count):
        def turn(i, carry):
            rows = rows_ref[i].astype(F32)
            fill = jnp.zeros((8 - n_layers, count), F32)
            place = pl.ds(pl.multiple_of(i * count, count), count)
            cols_ref[place, :] = jnp.concatenate([rows, fill], axis=0).T
            return carry

        lax.fori_loop(0, n_tp, turn, 0)

    steps = [(k, j) for k in range(ny) for j in range(nx)]
    right, left = lax.rem(s + 1, n_sp), lax.rem(s + n_sp - 1, n_sp)
    has_right, has_left = s < n_sp - 1, s > 0

    def rows_at(q, count):
        return pl.ds(pl.multiple_of(q * count, count), count)

    for l in range(n_layers):
        last = l + 1 == n_layers
        following = None if last else in_proj[l + 1]
        groups_of_rows = [pl.ds(m * group, group) for m in range(groups)]
        if l == 0:
            waiting = list(out_proj[0][1:])
            for d in range(1, nz):
                if d == nz - 1:
                    arrived(gain_copies)
                    to_columns(norm_rows, norm_cols, channels)
                    to_columns(out_rows, out_cols, features)
                for k in range(stream_pieces):
                    spread.step(d, k, cross.forward)
                    for way in ((1,) if d == 1 else (1, -1)):
                        cross.receive(way, d - 1, k)
                    if waiting and ((d - 1) * stream_pieces + k) % 2 == 1:
                        waiting.pop(0).send_x()
            for part in waiting:
                part.send_x()
            spread.wait_across()
            for d in range(1, nz):
                for way in (1, -1):
                    @pl.when(spread.has[way, d])
                    def _():
                        spread.wait_hand(way, d)
            for half, (parts, buf) in enumerate(zip(in_proj[l], (v_buf, g_buf))):
                total = None
                for k in range(ny):
                    for part in parts:
                        part.arrive(k, 0)
                    slot = slot_of(k, 0)
                    one = jnp.dot(buf[l, slot], h_all[l, rows_at(slot, f_cols), :], preferred_element_type=F32)
                    total = one if total is None else total + one
                acc[half] = total
            for k in range(stream_pieces):
                for way in (1, -1):
                    cross.receive(way, nz - 1, k)
            cross.finish()
            part_copies = {}
            for m, rows in enumerate(groups_of_rows):
                for j in range(1, nx):
                    for half, buf in enumerate((v_buf, g_buf)):
                        total = None
                        for k in range(ny):
                            block = rows_at(lax.rem(y + ny - k, ny), f_cols)
                            one = jnp.dot(
                                buf[l, slot_of(k, 0), rows, :], x_all[j - 1, block, :],
                                preferred_element_type=F32,
                            )
                            total = one if total is None else total + one
                        part_out[j - 1, half, rows, :] = total.astype(BF16)
                    copy = remote(
                        part_out.at[j - 1, :, rows, :], part_in.at[j - 1, :, rows, :],
                        y * nx + lax.rem(x + nx - j, nx), t,
                    )
                    start(copy)
                    part_copies[m, j] = copy
            for part in out_proj[0]:
                part.send_y()
        else:
            for part in in_proj[l][0] + in_proj[l][1]:
                part.flush()
            for k, j in steps:
                slot = slot_of(k, j)
                for half, (parts, buf) in enumerate(zip(in_proj[l], (v_buf, g_buf))):
                    for part in parts:
                        part.arrive(k, j)
                    one = jnp.dot(buf[l, slot], h_all[l, rows_at(slot, f_cols), :], preferred_element_type=F32)
                    if (k, j) == (0, 0):
                        acc[half] = one
                    else:
                        acc[half] += one

        edges = []
        for m, rows in enumerate(groups_of_rows):
            lanes = pl.ds(m * group, group)
            value, gate = acc[0, rows, :], acc[1, rows, :]
            if l == 0:
                for j in range(1, nx):
                    part_copies[m, j].wait_recv()
                    value = value + part_in[j - 1, 0, rows, :].astype(F32)
                    gate = gate + part_in[j - 1, 1, rows, :].astype(F32)
            gated = (value * jax.nn.sigmoid(gate)).astype(BF16)
            wide[l, pl.ds(EDGE, positions), lanes] = gated.astype(F32).T
            to_right = remote(
                wide.at[l, pl.ds(positions, EDGE), lanes], wide.at[l, pl.ds(0, EDGE), lanes], right, t
            )
            to_left = remote(
                wide.at[l, pl.ds(EDGE, EDGE), lanes], wide.at[l, pl.ds(EDGE + positions, EDGE), lanes], left, t
            )
            start(to_right, has_right)
            start(to_left, has_left)
            edges.append((to_right, to_left))

        if l == 0:
            if following is not None:
                following[0][0].send_x()
                for part in following[1] + following[0]:
                    part.send_y()
        if last:
            for part in out_proj[l]:
                part.send_x()

        blank = jnp.zeros((EDGE, channels), F32)

        @pl.when(s == 0)
        def _():
            wide[l, 0:EDGE, :] = blank

        @pl.when(s == n_sp - 1)
        def _():
            wide[l, EDGE + positions : 2 * EDGE + positions, :] = blank

        conv_size = channels // conv_pieces
        conv_spread = Spread(
            conv_all.at[l], channels, conv_pieces, rows_of(conv_all.at[l, my_channels, :], channels, conv_pieces)
        )
        own_sum = own_square = None
        for m in range(groups):
            lanes = pl.ds(m * group, group)
            to_right, to_left = edges[m]
            pl.when(has_left)(to_right.wait_recv)
            pl.when(has_right)(to_left.wait_recv)
            def conv_step(i, carry, lanes=lanes):
                first = pl.multiple_of(i * TILE, TILE)
                extent = TILE + 2 * EDGE
                window = wide[l, pl.ds(first, extent), lanes]
                total = None
                for r in range(8):
                    moved = window if r == 0 else pltpu.roll(window, extent - r, 0)
                    for q in range(0, 2 * EDGE + 1, 8):
                        tap = q + r - (EDGE - reach)
                        if 0 <= tap < n_taps:
                            term = tap_rows[l, tap : tap + 1, lanes] * moved[q : q + TILE]
                            total = term if total is None else total + term
                flat[pl.ds(first, TILE), lanes] = total
                return carry

            lax.fori_loop(0, positions // TILE, conv_step, 0)
            narrow = flat[:, lanes].T.astype(BF16)
            row = pl.multiple_of(t * channels + m * group, group)
            conv_all[l, pl.ds(row, group), :] = narrow
            for k in range(m * (group // conv_size), (m + 1) * (group // conv_size)):
                conv_spread.start_own(k)
            seen = narrow.astype(F32)
            part_sum = jnp.sum(seen, axis=0, keepdims=True)
            part_square = jnp.sum(seen * seen, axis=0, keepdims=True)
            own_sum = part_sum if own_sum is None else own_sum + part_sum
            own_square = part_square if own_square is None else own_square + part_square
        sums[l, t, 0:1, :] = own_sum
        sums[l, t, 1:2, :] = own_square
        sum_copies = exchange(sums.at[l, t], sums.at[l])

        turn = [None]

        def settle():
            arrived(sum_copies)
            totals = jnp.sum(sums[l], axis=0)
            average = totals[0:1] / width
            variance = totals[1:2] / width - average * average
            turn[0] = (average, lax.rsqrt(variance + 1e-05))

        def activate(block):
            average, inverse = turn[0]
            rows = rows_at(block, channels)
            gain = norm_cols[rows, l : l + 1]
            scaled = (conv_all[l, rows, :].astype(F32) - average) * inverse * gain
            active[rows, :] = (scaled / (1.0 + jnp.exp(-scaled))).astype(BF16)

        def drain(spread, ready, consume, hook):
            def take(d):
                for way in (1, -1):
                    @pl.when(spread.has[way, d])
                    def _():
                        consume((z - way * d) * 2 + c)
                        spread.wait_hand(way, d)
                        consume((z - way * d) * 2 + 1 - c)

            when = min(2, nz - 1)
            for d in range(1, nz):
                for k in range(spread.pieces):
                    spread.step(d, k)
                    hook((d - 1) * spread.pieces + k)
                if d == when:
                    ready()
                    consume(t)
                    spread.wait_across()
                    consume(z * 2 + 1 - c)
                if d >= when and d > 1:
                    take(d - 1)
            take(nz - 1)

        def conv_hook(i):
            if l == 0:
                if i == 1:
                    for part in out_proj[l][: out_parts // 2]:
                        part.relay()
                if i == 4:
                    for part in out_proj[l][out_parts // 2 :]:
                        part.relay()
                if i == 5 and following is not None:
                    following[0][1].send_x()
            if last and i % 3 == 0 and 0 < i // 3 <= out_parts:
                out_proj[l][i // 3 - 1].flush()

        drain(conv_spread, settle, activate, conv_hook)
        for part in out_proj[l]:
            part.flush()
        total = None
        for k, j in steps:
            slot = slot_of(k, j)
            for part in out_proj[l]:
                part.arrive(k, j)
            one = jnp.dot(o_buf[l, slot], active[rows_at(slot, c_cols), :], preferred_element_type=F32)
            total = one if total is None else total + one
        narrow_branch = total.astype(BF16)
        branch = narrow_branch.astype(F32)
        squares[l, t, 0:1, :] = jnp.sum(branch * branch, axis=0, keepdims=True)
        square_copies = exchange(squares.at[l, t], squares.at[l])

        def factor_of():
            arrived(square_copies)
            return lax.rsqrt(jnp.sum(squares[l], axis=0) / model + 1e-06)

        if last:
            factor = factor_of()
            gain = out_cols[my_rows, l : l + 1]
            fresh = h_all[l, my_rows, :].astype(F32) + branch * factor * gain
            result[...] = fresh.astype(BF16)
        else:
            branch_all[l, my_rows, :] = narrow_branch
            branch_spread = Spread(
                branch_all.at[l], features, stream_pieces,
                rows_of(branch_all.at[l, my_rows, :], features, stream_pieces),
            )
            for k in range(stream_pieces):
                branch_spread.start_own(k)
            if l == 0:
                for part in following[0] + following[1]:
                    part.send_x()

            factor = [None]

            def scale():
                factor[0] = factor_of()

            def renew(block):
                rows = rows_at(block, features)
                gain = out_cols[rows, l : l + 1]
                change = branch_all[l, rows, :].astype(F32) * factor[0] * gain
                h_all[l + 1, rows, :] = (h_all[l, rows, :].astype(F32) + change).astype(BF16)

            def branch_hook(i):
                if i == stream_pieces:
                    following[1][0].relay()
                    following[0][0].relay()
                if i == stream_pieces + 2:
                    following[1][1].relay()
                    following[0][1].relay()
                    for part in out_proj[l + 1]:
                        part.send_y()

            drain(branch_spread, scale, renew, branch_hook)

    for copy, condition in sent:
        if condition is None:
            copy.wait_send()
        else:
            pl.when(condition)(copy.wait_send)
    assert counter[0] <= send_sem.shape[0]
    assert local_count[0] <= local_sem.shape[0]


def copies_of(ny, nx, nz, layers, features, channels):
    n_sp, n_tp = ny * nx, 2 * nz
    stream_pieces = pieces_of(features, 128)
    groups = pieces_of(channels, LANES)
    conv_pieces = groups * pieces_of(channels // groups, 64)
    spread = 4 * (nz - 1) + 1
    weights = 2 * (ny - 1) + (n_sp - 1) * (4 * (layers - 1) + stream_pieces * layers)
    cross = (2 * nz - 1) * stream_pieces * 2 * (nx - 1)
    spreads = spread * (stream_pieces * layers + conv_pieces * layers)
    small = (n_tp - 1) * (2 + 2 * layers) + groups * (nx - 1) + 2 * groups * layers
    return weights + cross + spreads + small


def on_device(n_sp, n_tp, stream, value_weight, gate_weight, conv_taps, norm_gain, out_weight, out_gain):
    layers, channels, f_cols = value_weight.shape
    features, positions = stream.shape
    c_cols = out_weight.shape[2]
    ny, nx = grid_of(n_sp)
    copies = copies_of(ny, nx, n_tp // 2, layers, features, channels)
    vmem = pl.BlockSpec(memory_space=pltpu.VMEM)
    hbm = pl.BlockSpec(memory_space=pl.ANY)
    return pl.pallas_call(
        functools.partial(kernel, n_sp, n_tp, layers),
        out_shape=jax.ShapeDtypeStruct(stream.shape, BF16),
        in_specs=[hbm, hbm, hbm, vmem, vmem, hbm, vmem],
        out_specs=vmem,
        scratch_shapes=[
            pltpu.VMEM((layers, n_tp * features, positions), BF16),
            pltpu.VMEM((nx - 1, n_tp * features // nx, positions), BF16),
            pltpu.VMEM((layers, n_tp * channels, positions), BF16),
            pltpu.VMEM((max(layers - 1, 1), n_tp * features, positions), BF16),
            pltpu.VMEM((n_tp * channels, positions), BF16),
            pltpu.VMEM((layers, n_sp, channels, f_cols), BF16),
            pltpu.VMEM((layers, n_sp, channels, f_cols), BF16),
            pltpu.VMEM((layers, n_sp, features, c_cols), BF16),
            pltpu.VMEM((nx - 1, 2, channels, positions), BF16),
            pltpu.VMEM((nx - 1, 2, channels, positions), BF16),
            pltpu.VMEM((layers, positions + 2 * EDGE, channels), F32),
            pltpu.VMEM((positions, channels), F32),
            pltpu.VMEM((layers, 2 * EDGE, channels), F32),
            pltpu.VMEM((2, channels, positions), F32),
            pltpu.VMEM((layers, n_tp, 2, positions), F32),
            pltpu.VMEM((layers, n_tp, 1, positions), F32),
            pltpu.VMEM((n_tp, layers, channels), BF16),
            pltpu.VMEM((n_tp, layers, features), BF16),
            pltpu.VMEM((n_tp * channels, 8), F32),
            pltpu.VMEM((n_tp * features, 8), F32),
            pltpu.SemaphoreType.DMA((layers * (4 + 2 * pieces_of(features, 128)) + 1,)),
            pltpu.SemaphoreType.DMA((copies,)),
            pltpu.SemaphoreType.DMA((copies,)),
        ],
        compiler_params=pltpu.CompilerParams(
            collective_id=0, has_side_effects=True, vmem_limit_bytes=60 * 1024 * 1024
        ),
    )(stream, value_weight, gate_weight, conv_taps, norm_gain, out_weight, out_gain)


def solution(mesh):
    return jax.shard_map(
        functools.partial(on_device, mesh.shape["sp"], mesh.shape["tp"]),
        mesh=mesh,
        in_specs=(
            P("tp", "sp"),
            P(None, "tp", "sp"),
            P(None, "tp", "sp"),
            P(None, "tp", None),
            P(None, "tp"),
            P(None, "tp", "sp"),
            P(None, "tp"),
        ),
        out_specs=P("tp", "sp"),
        check_vma=False,
    )
```

time: 131 us -> 125 us (0.954)
  Pallas kernels: 128 us -> 121 us
    pallas_call x1, Pallas kernels: 128 us -> 121 us  [on_device(): pl.pallas_call(functools.partial(kernel, n_sp, n_tp, layers), out_shape=j...]
where the time goes in v1:
time: 125 us
  Pallas kernels  121 us (97%)
  local copies, waits for them, and re-layouts  3.21 us (3%)
    pallas_call x1, Pallas kernels, on_device(): pl.pallas_call(functools.partial(kernel, n_sp, n_tp, layers), out_shape=j...  121 us
    unnamed x2, local copies, waits for them, and re-layouts  3.21 us

profile of v1, /device:TPU:0, one launch (start us, length us, event | category | flops | bytes accessed | tf_op | source)
XLA Modules:
  0.0 124.7 jit_solution(14591957303496709387)
XLA Ops:
  0.0 1.5 %copy.8.taps = bf16[2,256,31]{2,1,0:T(8,128)(2,1)} copy(bf16[2,256,31]{1,0,2:T(2,128)(2,1)} %param.10) | data formatting | bytes 63488 | tf_op args[3]
  1.5 121.5 %shard_map.73 = bf16[512,256]{1,0:T(8,128)(2,1)} custom-call(bf16[512,256]{1,0:T(8,128)(2,1)} %stream.1, bf16[2,256,1024]{2,1,0:T(8,128)(2,1)} %value_w.1, bf16[2,256,1024]{2,1,0:T(8,128)(2,1)} %gate_w.1, bf16[2,256,31]{2,1,0:T(8,128)(2,1)} %copy.8.taps, bf16[2,256]{1,0:T(2,128)(2,1)} %norm_gain.1, bf16[2,512,512]{2,1,0:T(8,128)(2,1)} %out_w.1, ...), custom_call_target="tpu_custom_call" | custom-call | tf_op jit(solution)/shard_map/pallas_call | solution.py:624
  123.0 1.7 %copy.10 = bf16[512,256]{1,0:T(8,128)(2,1)} copy(bf16[512,256]{1,0:T(8,128)(2,1)} %shard_map.73) | data formatting | bytes 524288

commit v2 on v1

v2 whole, which is shorter than its diff:
```python
import functools

import jax
import jax.numpy as jnp
from jax import lax
from jax.experimental import pallas as pl
from jax.experimental.pallas import tpu as pltpu
from jax.sharding import PartitionSpec as P

MESH = pl.DeviceIdType.MESH
F32 = jnp.float32
BF16 = jnp.bfloat16
LANES = 128
EDGE = 16
TILE = 64


def grid_of(count):
    nx = int(count**0.5)
    while count % nx:
        nx -= 1
    return count // nx, nx


def pieces_of(rows, size):
    return max(1, rows // size)


def cuts_of(positions):
    inner = positions - 2 * EDGE
    count = max(1, inner // 64)
    size = inner // count // EDGE * EDGE
    cuts = [(EDGE + k * size, size) for k in range(count - 1)]
    first = EDGE + (count - 1) * size
    cuts.append((first, positions - EDGE - first))
    return cuts


def kernel(
    n_sp, n_tp, n_layers,
    stream, value_w, gate_w, taps, norm_gain, out_w, out_gain,
    result,
    h_all, x_all, conv_all, conv_edge, branch_all, active, v_buf, g_buf, o_buf, part_out, part_in, wide, stat_cols, tap_rows,
    acc, sums, squares, norm_rows, out_rows, out_cols,
    local_sem, send_sem, recv_sem,
):
    ny, nx = grid_of(n_sp)
    nz = n_tp // 2
    s, t = lax.axis_index("sp"), lax.axis_index("tp")
    y, x = s // nx, s % nx
    z, c = t // 2, t % 2
    features, positions = stream.shape
    channels = value_w.shape[1]
    f_cols = value_w.shape[2]
    c_cols = out_w.shape[2]
    width = channels * n_tp
    model = features * n_tp
    n_taps = taps.shape[0]
    reach = n_taps // 2
    groups = pieces_of(channels, LANES)
    group = channels // groups
    sends, recvs, sent = [0], [0], []

    def send_slot():
        sends[0] += 1
        return sends[0] - 1

    def recv_slot(count=1):
        recvs[0] += count
        return recvs[0] - count

    def remote(src, dst, sp, tp, send=None, recv=None):
        return pltpu.make_async_remote_copy(
            src_ref=src, dst_ref=dst,
            send_sem=send_sem.at[0 if send is None else send], recv_sem=recv_sem.at[0 if recv is None else recv],
            device_id={"sp": sp, "tp": tp}, device_id_type=MESH,
        )

    def start(copy, condition=None):
        if condition is None:
            copy.start()
        else:
            pl.when(condition)(copy.start)

    def leave(ref, send, condition=None):
        sent.append((remote(ref, ref, s, t, send=send), condition))

    def slot_of(k, j):
        return lax.rem(y + ny - k, ny) * nx + lax.rem(x + nx - j, nx)

    def x_peer(j):
        return y * nx + lax.rem(x + j, nx)

    def y_peer(k):
        return lax.rem(y + k, ny) * nx + x

    local_count = [0]

    def local_copy(src, dst):
        i = local_count[0]
        local_count[0] += 1
        copy = pltpu.make_async_copy(src, dst, local_sem.at[i])
        copy.start()
        return copy

    class Gather:
        def __init__(self, src, dst, x_first, whole, send):
            self.copies, self.own_x, self.own_y, self.relays = {}, [], [], []
            for k in range(ny):
                for j in range(nx if whole else 1):
                    if k == 0 and j == 0:
                        continue
                    if x_first:
                        along_x = k == 0
                        origin = (0, 0) if along_x else (0, j)
                    else:
                        along_x = j > 0
                        origin = (k, 0) if along_x else (0, 0)
                    own = origin == (0, 0)
                    target = x_peer(j) if along_x else y_peer(k)
                    origin_slot = slot_of(*origin)
                    copy = remote(
                        src if own else dst(origin_slot), dst(origin_slot), target, t, send=send, recv=recv_slot()
                    )
                    self.copies[k, j] = copy
                    if not own:
                        self.relays.append((copy, origin))
                    elif along_x:
                        self.own_x.append(copy)
                    else:
                        self.own_y.append(copy)
            self.local = local_copy(src, dst(s))
            self.here, self.done = set(), set()

        def once(self, name):
            fresh = name not in self.done
            self.done.add(name)
            return fresh

        def send_x(self):
            if self.once("x"):
                for copy in self.own_x:
                    start(copy)

        def send_y(self):
            if self.once("y"):
                for copy in self.own_y:
                    start(copy)

        def relay(self):
            if self.once("relay"):
                for copy, origin in self.relays:
                    self.arrive(*origin)
                    start(copy)

        def flush(self):
            self.send_x()
            self.send_y()
            self.relay()

        def arrive(self, k, j):
            if (k, j) not in self.here:
                self.here.add((k, j))
                if k == 0 and j == 0:
                    self.local.wait()
                else:
                    self.copies[k, j].wait_recv()

    def gathers(w_ref, buf, l, orders, whole=True):
        rows = w_ref.shape[1] // len(orders)
        made, send = [], send_slot()
        leave(buf.at[l, pl.ds(0, (n_sp if whole else ny) - 1)], send)
        for i, x_first in enumerate(orders):
            part = pl.ds(i * rows, rows)
            made.append(Gather(w_ref.at[l, part], lambda q, part=part: buf.at[l, q, part], x_first, whole, send))
        return made

    class Spread:
        def __init__(self, pieces, at, whole, direct=False):
            def place(zz, cc, k):
                return at(jnp.clip(zz, 0, nz - 1) * 2 + cc, k)

            def full(zz, cc):
                return whole(jnp.clip(zz, 0, nz - 1) * 2 + cc)

            other = z * 2 + 1 - c
            self.pieces, self.place, self.direct = pieces, place, direct
            send, recv = send_slot(), recv_slot()
            self.across = [
                remote(place(z, c, k), place(z, c, k), s, other, send, recv) for k in range(pieces)
            ]
            self.landed = remote(full(z, 1 - c), full(z, 1 - c), s, other, recv=recv)
            leave(full(z, c), send)
            self.along, self.goes, self.hand, self.has, self.handed = {}, {}, {}, {}, {}
            for d in range(1, nz):
                for way in (1, -1):
                    has = (z - way * d >= 0) & (z - way * d < nz)
                    self.has[way, d] = has
                    send, hand_send, hand_recv = send_slot(), send_slot(), recv_slot()
                    if direct:
                        from_z, to_z = z, z + way * d
                        self.goes[way, d] = (to_z >= 0) & (to_z < nz)
                    else:
                        from_z, to_z = z - way * (d - 1), z + way
                        self.goes[way, d] = (from_z >= 0) & (from_z < nz) & (to_z >= 0) & (to_z < nz)
                    target = jnp.clip(to_z, 0, nz - 1) * 2 + c
                    for k in range(pieces):
                        held = place(from_z, c, k)
                        self.along[way, d, k] = remote(held, held, s, target, send, recv_slot())
                        seen = place(z - way * d, c, k)
                        self.hand[way, d, k] = remote(seen, seen, s, other, hand_send, hand_recv)
                    block = full(z - way * d, c)
                    self.handed[way, d] = remote(block, block, s, other, recv=hand_recv)
                    leave(block, send, self.goes[way, d])
                    leave(block, hand_send, has)

        def send(self, way, d, k):
            start(self.along[way, d, k], self.goes[way, d])

        def start_own(self, k):
            for d in range(1, nz) if self.direct else (1,):
                for way in (1, -1):
                    self.send(way, d, k)
            start(self.across[k])

        def step(self, d, k, extra=None):
            for way in (1, -1):
                pl.when(self.has[way, d])(self.along[way, d, k].wait_recv)
                if d + 1 < nz and not self.direct:
                    self.send(way, d + 1, k)
                start(self.hand[way, d, k], self.has[way, d])
                if extra is not None:
                    extra(way, d, k)

        def wait_across(self):
            self.landed.wait_recv()

        def wait_hand(self, way, d):
            self.handed[way, d].wait_recv()

    class Cross:
        def __init__(self, spread):
            self.spread = spread
            self.size = features // spread.pieces
            self.sends, self.base, self.hands = {}, {}, {}

        def facts(self, way, d):
            zz = z - way * d
            ok = (zz >= 0) & (zz < nz)
            q = jnp.clip(zz, 0, nz - 1)
            return ok, q, lax.rem(q, nx)

        def rows(self, q, k, count=1):
            size = self.size
            row = (q // nx * 2 + c) * features + k * size
            return pl.ds(pl.multiple_of(row, size), size * count)

        def forward(self, way, d, k):
            ok, q, owner = self.facts(way, d)
            pick = jnp.clip(lax.rem(owner - x + nx, nx) - 1, 0, nx - 2)
            if (way, d) not in self.sends:
                self.sends[way, d] = send_slot()
                leave(x_all.at[0, self.rows(q, 0, self.spread.pieces), :], self.sends[way, d], ok & (owner != x))
            base = self.base[way, d, k] = recv_slot(nx - 1)
            copy = remote(
                self.spread.place(q, c, k), x_all.at[pick, self.rows(q, k), :], y * nx + owner, t,
                self.sends[way, d], base + pick,
            )
            start(copy, ok & (owner != x))

        def receive(self, way, d, k):
            ok, q, owner = self.facts(way, d)
            mine = ok & (owner == x)
            for j in range(1, nx):
                if k == 0:
                    block = x_all.at[j - 1, self.rows(q, 0, self.spread.pieces), :]
                    send, recv = send_slot(), recv_slot()
                    self.hands[way, d, j] = (send, recv, remote(block, block, s, t, recv=recv), mine)
                    leave(block, send, mine)
                send, recv, _, _ = self.hands[way, d, j]
                here = x_all.at[j - 1, self.rows(q, k), :]
                landed = remote(here, here, s, t, recv=self.base[way, d, k] + j - 1)
                pl.when(mine)(landed.wait_recv)
                start(remote(here, here, s, z * 2 + 1 - c, send, recv), mine)

        def finish(self):
            for _, _, handed, mine in self.hands.values():
                pl.when(mine)(handed.wait_recv)

    def exchange(src, buf):
        send, recv = send_slot(), recv_slot()
        others = buf.at[pl.ds(0, n_tp - 1)]
        for k in range(1, n_tp):
            start(remote(src, buf.at[t], s, lax.rem(t + k, n_tp), send, recv))
        leave(others, send)
        return [remote(others, others, s, t, recv=recv)]

    def arrived(copies):
        for copy in copies:
            copy.wait_recv()

    my_rows = pl.ds(pl.multiple_of(t * features, features), features)
    stream_pieces = pieces_of(features, 128)
    cuts = cuts_of(positions)

    def row_spread(buf):
        size = features // stream_pieces

        def at(block, k):
            return buf.at[pl.ds(pl.multiple_of(block * features + k * size, size), size), :]

        def whole(block):
            return buf.at[pl.ds(pl.multiple_of(block * features, features), features), :]

        return Spread(stream_pieces, at, whole)

    def position_spreads(inner, edge):
        return (
            Spread(
                len(cuts), lambda block, k: inner.at[block, pl.ds(cuts[k][0], cuts[k][1]), :],
                lambda block: inner.at[block, pl.ds(EDGE, positions - 2 * EDGE), :],
            ),
            Spread(1, lambda block, k: edge.at[block], lambda block: edge.at[block], direct=True),
        )

    stream_copy = local_copy(stream, h_all.at[0, my_rows, :])
    barrier = pltpu.get_barrier_semaphore()
    for k in range(1, n_sp):
        pl.semaphore_signal(
            barrier, inc=1, device_id={"sp": lax.rem(s + k, n_sp), "tp": t}, device_id_type=MESH
        )
    for k in range(1, n_tp):
        pl.semaphore_signal(
            barrier, inc=1, device_id={"sp": s, "tp": lax.rem(t + k, n_tp)}, device_id_type=MESH
        )
    in_proj, out_proj = [], []
    out_parts = pieces_of(features, 128)
    for l in range(n_layers):
        if l == 0:
            v_parts = gathers(value_w, v_buf, l, [True], whole=False)
            g_parts = gathers(gate_w, g_buf, l, [True], whole=False)
        else:
            v_parts = gathers(value_w, v_buf, l, [True, True])
            g_parts = gathers(gate_w, g_buf, l, [False, False])
        in_proj.append((v_parts, g_parts))
        last = l + 1 == n_layers
        out_proj.append(gathers(out_w, o_buf, l, [last] * out_parts))
    norm_rows[t] = norm_gain[...]
    out_rows[t] = out_gain[...]
    for l in range(n_layers):
        tap_rows[l, 0:n_taps, :] = taps[:, l, :].astype(F32)
    stream_copy.wait()
    pl.semaphore_wait(barrier, n_sp + n_tp - 2)

    spread = row_spread(h_all.at[0])
    cross = Cross(spread)
    for k in range(stream_pieces):
        spread.start_own(k)
        cross.forward(1, 0, k)
    for part in in_proj[0][0] + in_proj[0][1]:
        part.send_y()
    out_proj[0][0].send_x()
    gain_copies = exchange(norm_gain, norm_rows) + exchange(out_gain, out_rows)

    def turn_gain(i):
        rows = out_rows[i].astype(F32)
        fill = jnp.zeros((8 - n_layers, features), F32)
        out_cols[i * features : (i + 1) * features, :] = jnp.concatenate([rows, fill], axis=0).T

    def across_lanes(a, b):
        return lax.dot_general(a, b, (((1,), (1,)), ((), ())), preferred_element_type=F32)

    turned = [0]
    steps = [(k, j) for k in range(ny) for j in range(nx)]
    right, left = lax.rem(s + 1, n_sp), lax.rem(s + n_sp - 1, n_sp)
    has_right, has_left = s < n_sp - 1, s > 0

    def rows_at(q, count):
        return pl.ds(pl.multiple_of(q * count, count), count)

    for l in range(n_layers):
        last = l + 1 == n_layers
        following = None if last else in_proj[l + 1]
        groups_of_rows = [pl.ds(m * group, group) for m in range(groups)]
        if l == 0:
            waiting = list(out_proj[0][1:])
            for d in range(1, nz):
                for k in range(stream_pieces):
                    spread.step(d, k, cross.forward)
                    for way in ((1,) if d == 1 else (1, -1)):
                        cross.receive(way, d - 1, k)
                    if waiting and ((d - 1) * stream_pieces + k) % 2 == 1:
                        waiting.pop(0).send_x()
            for part in waiting:
                part.send_x()
            spread.wait_across()
            for d in range(1, nz):
                for way in (1, -1):
                    @pl.when(spread.has[way, d])
                    def _():
                        spread.wait_hand(way, d)
            for half, (parts, buf) in enumerate(zip(in_proj[l], (v_buf, g_buf))):
                total = None
                for k in range(ny):
                    for part in parts:
                        part.arrive(k, 0)
                    slot = slot_of(k, 0)
                    one = jnp.dot(buf[l, slot], h_all[l, rows_at(slot, f_cols), :], preferred_element_type=F32)
                    total = one if total is None else total + one
                acc[half] = total
            for k in range(stream_pieces):
                for way in (1, -1):
                    cross.receive(way, nz - 1, k)
            cross.finish()
            part_copies = {}
            for m, rows in enumerate(groups_of_rows):
                for j in range(1, nx):
                    for half, buf in enumerate((v_buf, g_buf)):
                        total = None
                        for k in range(ny):
                            block = rows_at(lax.rem(y + ny - k, ny), f_cols)
                            one = jnp.dot(
                                buf[l, slot_of(k, 0), rows, :], x_all[j - 1, block, :],
                                preferred_element_type=F32,
                            )
                            total = one if total is None else total + one
                        part_out[j - 1, half, rows, :] = total.astype(BF16)
                    mine = part_out.at[j - 1, :, rows, :]
                    send = send_slot()
                    copy = remote(
                        mine, part_in.at[j - 1, :, rows, :], y * nx + lax.rem(x + nx - j, nx), t,
                        send, recv_slot(),
                    )
                    start(copy)
                    leave(mine, send)
                    part_copies[m, j] = copy
            for part in out_proj[0]:
                part.send_y()
        else:
            for part in in_proj[l][0] + in_proj[l][1]:
                part.flush()
            for k, j in steps:
                slot = slot_of(k, j)
                for half, (parts, buf) in enumerate(zip(in_proj[l], (v_buf, g_buf))):
                    for part in parts:
                        part.arrive(k, j)
                    one = jnp.dot(buf[l, slot], h_all[l, rows_at(slot, f_cols), :], preferred_element_type=F32)
                    if (k, j) == (0, 0):
                        acc[half] = one
                    else:
                        acc[half] += one

        edges = []
        for m, rows in enumerate(groups_of_rows):
            lanes = pl.ds(m * group, group)
            value, gate = acc[0, rows, :], acc[1, rows, :]
            if l == 0:
                for j in range(1, nx):
                    part_copies[m, j].wait_recv()
                    value = value + part_in[j - 1, 0, rows, :].astype(F32)
                    gate = gate + part_in[j - 1, 1, rows, :].astype(F32)
            gated = (value * jax.nn.sigmoid(gate)).astype(BF16)
            wide[l, pl.ds(EDGE, positions), lanes] = gated.astype(F32).T
            pair = []
            for first, land, peer, here in (
                (positions, 0, right, has_right), (EDGE, EDGE + positions, left, has_left)
            ):
                mine, send = wide.at[l, pl.ds(first, EDGE), lanes], send_slot()
                copy = remote(mine, wide.at[l, pl.ds(land, EDGE), lanes], peer, t, send, recv_slot())
                start(copy, here)
                leave(mine, send, here)
                pair.append(copy)
            to_right, to_left = pair
            edges.append((to_right, to_left))

        if l == 0:
            if following is not None:
                following[0][0].send_x()
                for part in following[1] + following[0]:
                    part.send_y()
        if last:
            for part in out_proj[l]:
                part.send_x()

        blank = jnp.zeros((EDGE, channels), F32)

        @pl.when(s == 0)
        def _():
            wide[l, 0:EDGE, :] = blank

        @pl.when(s == n_sp - 1)
        def _():
            wide[l, EDGE + positions : 2 * EDGE + positions, :] = blank

        def convolve(first, count, dst, land):
            while count:
                size = min(TILE, count)
                for m in range(groups):
                    lanes = pl.ds(m * group, group)
                    extent = size + 2 * EDGE
                    window = wide[l, pl.ds(first, extent), lanes]
                    total = None
                    for r in range(8):
                        moved = window if r == 0 else pltpu.roll(window, extent - r, 0)
                        for q in range(0, 2 * EDGE + 1, 8):
                            tap = q + r - (EDGE - reach)
                            if 0 <= tap < n_taps:
                                term = tap_rows[l, tap : tap + 1, lanes] * moved[q : q + size]
                                total = term if total is None else total + term
                    dst[l, t, pl.ds(land, size), lanes] = total.astype(BF16)
                first, land, count = first + size, land + size, count - size

        def total_up(phase, seen):
            square = seen.astype(F32) * seen.astype(F32)
            high = square.astype(BF16)
            low = (square - high.astype(F32)).astype(BF16)
            ones = jnp.ones((8, channels), BF16)
            sums[l, phase, t, 0:1, :] = across_lanes(ones, seen)[0:1]
            sums[l, phase, t, 1:2, :] = (across_lanes(ones, high) + across_lanes(ones, low))[0:1]
            return exchange(sums.at[l, phase, t], sums.at[l, phase])

        inner, edge = position_spreads(conv_all.at[l], conv_edge.at[l])
        border = jnp.zeros((EDGE, channels), BF16)
        conv_all[l, t, 0:EDGE, :] = border
        conv_all[l, t, positions - EDGE : positions, :] = border
        for k, (first, count) in enumerate(cuts):
            convolve(first, count, conv_all, first)
            inner.start_own(k)
        sum_copies = [total_up(0, conv_all[l, t]), None]

        def finish_edges():
            for to_right, to_left in edges:
                pl.when(has_left)(to_right.wait_recv)
                pl.when(has_right)(to_left.wait_recv)
            convolve(0, EDGE, conv_edge, 0)
            convolve(positions - EDGE, EDGE, conv_edge, EDGE)
            edge.start_own(0)
            conv_all[l, t, 0:EDGE, :] = conv_edge[l, t, 0:EDGE, :]
            conv_all[l, t, positions - EDGE : positions, :] = conv_edge[l, t, EDGE : 2 * EDGE, :]
            sum_copies[1] = total_up(1, conv_all[l, t])

        def settle(phase):
            arrived(sum_copies[phase])
            totals = jnp.sum(sums[l, phase], axis=0)
            average = totals[0:1] / width
            variance = totals[1:2] / width - average * average
            for i, row in enumerate((average, lax.rsqrt(variance + 1e-05))):
                column = jnp.broadcast_to(row, (LANES, positions)).T
                if channels > LANES:
                    column = jnp.concatenate([column] * (channels // LANES), axis=1)
                stat_cols[i] = column[:, :channels]

        def activate(src, block, first, count, land):
            gain = norm_rows[block].astype(F32)[l : l + 1]
            place = pl.ds(land, count)
            seen = src[l, block, pl.ds(first, count), :].astype(F32)
            scaled = (seen - stat_cols[0, place, :]) * stat_cols[1, place, :] * gain
            active[block, place, :] = (scaled / (1.0 + jnp.exp(-scaled))).astype(BF16)

        def activate_inner(block):
            activate(conv_all, block, EDGE, positions - 2 * EDGE, EDGE)

        def drain(spread, ready, consume, hook, finish=None):
            def take(d):
                for way in (1, -1):
                    @pl.when(spread.has[way, d])
                    def _():
                        consume((z - way * d) * 2 + c)
                        spread.wait_hand(way, d)
                        consume((z - way * d) * 2 + 1 - c)

            when = min(2, nz - 1)
            for d in range(1, nz):
                for k in range(spread.pieces):
                    spread.step(d, k)
                    hook((d - 1) * spread.pieces + k)
                if d == when:
                    ready()
                    consume(t)
                    spread.wait_across()
                    consume(z * 2 + 1 - c)
                if d >= when and d > 1:
                    take(d - 1)
            if finish is not None:
                finish()
            take(nz - 1)

        def conv_hook(i):
            if i == min(1, len(cuts) - 1):
                finish_edges()
            if l == 0:
                if i == 2:
                    arrived(gain_copies)
                if i >= 2 and turned[0] < n_tp:
                    turn_gain(turned[0])
                    turned[0] += 1
                if i == 1:
                    for part in out_proj[l][: out_parts // 2]:
                        part.relay()
                if i == 4:
                    for part in out_proj[l][out_parts // 2 :]:
                        part.relay()
                if i == 5 and following is not None:
                    following[0][1].send_x()
            if last and i % 3 == 0 and 0 < i // 3 <= out_parts:
                out_proj[l][i // 3 - 1].flush()

        def catch_edges():
            for d in range(1, nz):
                edge.step(d, 0)

        drain(inner, lambda: settle(0), activate_inner, conv_hook, catch_edges)
        edge.wait_across()
        for d in range(1, nz):
            for way in (1, -1):
                @pl.when(edge.has[way, d])
                def _():
                    edge.wait_hand(way, d)
        settle(1)
        for block in range(n_tp):
            activate(conv_edge, block, 0, EDGE, 0)
            activate(conv_edge, block, EDGE, EDGE, positions - EDGE)
        while turned[0] < n_tp:
            turn_gain(turned[0])
            turned[0] += 1
        for part in out_proj[l]:
            part.flush()
        total = None
        for k, j in steps:
            slot = slot_of(k, j)
            for part in out_proj[l]:
                part.arrive(k, j)
            for i in range(c_cols // channels):
                one = across_lanes(
                    o_buf[l, slot, :, i * channels : (i + 1) * channels], active[slot * (c_cols // channels) + i]
                )
                total = one if total is None else total + one
        narrow_branch = total.astype(BF16)
        branch = narrow_branch.astype(F32)
        squares[l, t, 0:1, :] = jnp.sum(branch * branch, axis=0, keepdims=True)
        square_copies = exchange(squares.at[l, t], squares.at[l])

        def factor_of():
            arrived(square_copies)
            return lax.rsqrt(jnp.sum(squares[l], axis=0) / model + 1e-06)

        if last:
            factor = factor_of()
            gain = out_cols[my_rows, l : l + 1]
            fresh = h_all[l, my_rows, :].astype(F32) + branch * factor * gain
            result[...] = fresh.astype(BF16)
        else:
            branch_all[l, my_rows, :] = narrow_branch
            branch_spread = row_spread(branch_all.at[l])
            for k in range(stream_pieces):
                branch_spread.start_own(k)
            if l == 0:
                for part in following[0] + following[1]:
                    part.send_x()

            factor = [None]

            def scale():
                factor[0] = factor_of()

            def renew(block):
                rows = rows_at(block, features)
                gain = out_cols[rows, l : l + 1]
                change = branch_all[l, rows, :].astype(F32) * factor[0] * gain
                h_all[l + 1, rows, :] = (h_all[l, rows, :].astype(F32) + change).astype(BF16)

            def branch_hook(i):
                if i == stream_pieces:
                    following[1][0].relay()
                    following[0][0].relay()
                if i == stream_pieces + 2:
                    following[1][1].relay()
                    following[0][1].relay()
                    for part in out_proj[l + 1]:
                        part.send_y()

            drain(branch_spread, scale, renew, branch_hook)

    for copy, condition in sent:
        if condition is None:
            copy.wait_send()
        else:
            pl.when(condition)(copy.wait_send)
    assert sends[0] == send_sem.shape[0], sends
    assert recvs[0] == recv_sem.shape[0], recvs
    assert local_count[0] == local_sem.shape[0], local_count


def slots_of(ny, nx, nz, layers, features, channels, positions):
    n_sp, far = ny * nx, 2 * (nz - 1)
    pieces, cuts, groups = pieces_of(features, 128), len(cuts_of(positions)), pieces_of(channels, LANES)
    small = 2 + 3 * layers + groups * (nx - 1) + 2 * groups * layers
    send = 3 * layers * (1 + 2 * far) + (far + 1) * nx + 3 * layers + small
    recv = layers * (3 + far * (pieces + 1 + cuts + 1 + 2)) + (far + 1) * (pieces + 1) * (nx - 1)
    recv += 2 * (ny - 1) + (n_sp - 1) * (4 * (layers - 1) + pieces * layers) + small
    local = 1 + 2 + 4 * (layers - 1) + pieces * layers
    return send, recv, local


def on_device(n_sp, n_tp, stream, value_weight, gate_weight, conv_taps, norm_gain, out_weight, out_gain):
    layers, channels, f_cols = value_weight.shape
    features, positions = stream.shape
    c_cols = out_weight.shape[2]
    ny, nx = grid_of(n_sp)
    send, recv, local = slots_of(ny, nx, n_tp // 2, layers, features, channels, positions)
    vmem = pl.BlockSpec(memory_space=pltpu.VMEM)
    hbm = pl.BlockSpec(memory_space=pl.ANY)
    return pl.pallas_call(
        functools.partial(kernel, n_sp, n_tp, layers),
        out_shape=jax.ShapeDtypeStruct(stream.shape, BF16),
        in_specs=[hbm, hbm, hbm, vmem, vmem, hbm, vmem],
        out_specs=vmem,
        scratch_shapes=[
            pltpu.VMEM((layers, n_tp * features, positions), BF16),
            pltpu.VMEM((nx - 1, n_tp * features // nx, positions), BF16),
            pltpu.VMEM((layers, n_tp, positions, channels), BF16),
            pltpu.VMEM((layers, n_tp, 2 * EDGE, channels), BF16),
            pltpu.VMEM((max(layers - 1, 1), n_tp * features, positions), BF16),
            pltpu.VMEM((n_tp, positions, channels), BF16),
            pltpu.VMEM((layers, n_sp, channels, f_cols), BF16),
            pltpu.VMEM((layers, n_sp, channels, f_cols), BF16),
            pltpu.VMEM((layers, n_sp, features, c_cols), BF16),
            pltpu.VMEM((nx - 1, 2, channels, positions), BF16),
            pltpu.VMEM((nx - 1, 2, channels, positions), BF16),
            pltpu.VMEM((layers, positions + 2 * EDGE, channels), F32),
            pltpu.VMEM((2, positions, channels), F32),
            pltpu.VMEM((layers, 2 * EDGE, channels), F32),
            pltpu.VMEM((2, channels, positions), F32),
            pltpu.VMEM((layers, 2, n_tp, 2, positions), F32),
            pltpu.VMEM((layers, n_tp, 1, positions), F32),
            pltpu.VMEM((n_tp, layers, channels), BF16),
            pltpu.VMEM((n_tp, layers, features), BF16),
            pltpu.VMEM((n_tp * features, 8), F32),
            pltpu.SemaphoreType.DMA((local,)),
            pltpu.SemaphoreType.DMA((send,)),
            pltpu.SemaphoreType.DMA((recv,)),
        ],
        compiler_params=pltpu.CompilerParams(
            collective_id=0, has_side_effects=True, vmem_limit_bytes=60 * 1024 * 1024
        ),
    )(stream, value_weight, gate_weight, jnp.transpose(conv_taps, (2, 0, 1)), norm_gain, out_weight, out_gain)


def solution(mesh):
    return jax.shard_map(
        functools.partial(on_device, mesh.shape["sp"], mesh.shape["tp"]),
        mesh=mesh,
        in_specs=(
            P("tp", "sp"),
            P(None, "tp", "sp"),
            P(None, "tp", "sp"),
            P(None, "tp", None),
            P(None, "tp"),
            P(None, "tp", "sp"),
            P(None, "tp"),
        ),
        out_specs=P("tp", "sp"),
        check_vma=False,
    )
```

time: 125 us -> 120 us (0.960)
  Pallas kernels: 121 us -> 117 us
  local copies, waits for them, and re-layouts: 3.21 us -> 1.67 us
    pallas_call x1, Pallas kernels: 121 us -> 117 us  [on_device(): pl.pallas_call(functools.partial(kernel, n_sp, n_tp, layers), out_shape=j...]
    unnamed x2 -> x1, local copies, waits for them, and re-layouts: 3.21 us -> 1.67 us
where the time goes in v2:
time: 120 us; the launch traced here: 119 us
  Pallas kernels  117 us (98%)
  local copies, waits for them, and re-layouts  1.67 us (1%)
    pallas_call x1, Pallas kernels, on_device(): pl.pallas_call(functools.partial(kernel, n_sp, n_tp, layers), out_shape=j...  117 us

profile of v2, /device:TPU:0, one launch (start us, length us, event | category | flops | bytes accessed | tf_op | source)
XLA Modules:
  0.0 119.1 jit_solution(8366057045141974114)
XLA Ops:
  0.0 117.4 %shard_map.73 = bf16[512,256]{1,0:T(8,128)(2,1)} custom-call(bf16[512,256]{1,0:T(8,128)(2,1)} %stream.1, bf16[2,256,1024]{2,1,0:T(8,128)(2,1)} %value_w.1, bf16[2,256,1024]{2,1,0:T(8,128)(2,1)} %gate_w.1, bf16[31,2,256]{2,1,0:T(2,128)(2,1)} %bitcast.1, bf16[2,256]{1,0:T(2,128)(2,1)} %norm_gain.1, bf16[2,512,512]{2,1,0:T(8,128)(2,1)} %out_w.1, ...), custom_call_target="tpu_custom_call" | custom-call | tf_op jit(solution)/shard_map/pallas_call | solution.py:713
  117.4 1.7 %copy.9 = bf16[512,256]{1,0:T(8,128)(2,1)} copy(bf16[512,256]{1,0:T(8,128)(2,1)} %shard_map.73) | data formatting | bytes 524288

commit v3 on v2

--- a/solution.py
+++ b/solution.py
@@ -40,7 +40,7 @@
     n_sp, n_tp, n_layers,
     stream, value_w, gate_w, taps, norm_gain, out_w, out_gain,
     result,
-    h_all, x_all, conv_all, conv_edge, branch_all, active, v_buf, g_buf, o_buf, part_out, part_in, wide, stat_cols, tap_rows,
+    h_all, x_all, x_branch, own_factor, peer_factor, conv_all, conv_edge, branch_all, active, v_buf, g_buf, o_buf, part_out, part_in, wide, stat_cols, tap_rows,
     acc, sums, squares, norm_rows, out_rows, out_cols,
     local_sem, send_sem, recv_sem,
 ):
@@ -239,8 +239,8 @@
             self.handed[way, d].wait_recv()
 
     class Cross:
-        def __init__(self, spread):
-            self.spread = spread
+        def __init__(self, spread, land):
+            self.spread, self.land = spread, land
             self.size = features // spread.pieces
             self.sends, self.base, self.hands = {}, {}, {}
 
@@ -260,10 +260,10 @@
             pick = jnp.clip(lax.rem(owner - x + nx, nx) - 1, 0, nx - 2)
             if (way, d) not in self.sends:
                 self.sends[way, d] = send_slot()
-                leave(x_all.at[0, self.rows(q, 0, self.spread.pieces), :], self.sends[way, d], ok & (owner != x))
+                leave(self.land.at[0, self.rows(q, 0, self.spread.pieces), :], self.sends[way, d], ok & (owner != x))
             base = self.base[way, d, k] = recv_slot(nx - 1)
             copy = remote(
-                self.spread.place(q, c, k), x_all.at[pick, self.rows(q, k), :], y * nx + owner, t,
+                self.spread.place(q, c, k), self.land.at[pick, self.rows(q, k), :], y * nx + owner, t,
                 self.sends[way, d], base + pick,
             )
             start(copy, ok & (owner != x))
@@ -273,12 +273,12 @@
             mine = ok & (owner == x)
             for j in range(1, nx):
                 if k == 0:
-                    block = x_all.at[j - 1, self.rows(q, 0, self.spread.pieces), :]
+                    block = self.land.at[j - 1, self.rows(q, 0, self.spread.pieces), :]
                     send, recv = send_slot(), recv_slot()
                     self.hands[way, d, j] = (send, recv, remote(block, block, s, t, recv=recv), mine)
                     leave(block, send, mine)
                 send, recv, _, _ = self.hands[way, d, j]
-                here = x_all.at[j - 1, self.rows(q, k), :]
+                here = self.land.at[j - 1, self.rows(q, k), :]
                 landed = remote(here, here, s, t, recv=self.base[way, d, k] + j - 1)
                 pl.when(mine)(landed.wait_recv)
                 start(remote(here, here, s, z * 2 + 1 - c, send, recv), mine)
@@ -336,15 +336,9 @@
     in_proj, out_proj = [], []
     out_parts = pieces_of(features, 128)
     for l in range(n_layers):
-        if l == 0:
-            v_parts = gathers(value_w, v_buf, l, [True], whole=False)
-            g_parts = gathers(gate_w, g_buf, l, [True], whole=False)
-        else:
-            v_parts = gathers(value_w, v_buf, l, [True, True])
-            g_parts = gathers(gate_w, g_buf, l, [False, False])
-        in_proj.append((v_parts, g_parts))
+        in_proj.append(gathers(value_w, v_buf, l, [True], False) + gathers(gate_w, g_buf, l, [True], False))
         last = l + 1 == n_layers
-        out_proj.append(gathers(out_w, o_buf, l, [last] * out_parts))
+        out_proj.append(gathers(out_w, o_buf, l, [last and i % 2 == 0 for i in range(out_parts)]))
     norm_rows[t] = norm_gain[...]
     out_rows[t] = out_gain[...]
     for l in range(n_layers):
@@ -353,13 +347,18 @@
     pl.semaphore_wait(barrier, n_sp + n_tp - 2)
 
     spread = row_spread(h_all.at[0])
-    cross = Cross(spread)
+    cross = Cross(spread, x_all.at[0])
     for k in range(stream_pieces):
         spread.start_own(k)
         cross.forward(1, 0, k)
-    for part in in_proj[0][0] + in_proj[0][1]:
+    early = max(1, out_parts // 2)
+    for part in out_proj[0][:early]:
+        part.send_x()
+    for part in in_proj[0] + out_proj[0]:
         part.send_y()
-    out_proj[0][0].send_x()
+    for l in range(1, n_layers):
+        for part in in_proj[l]:
+            part.send_y()
     gain_copies = exchange(norm_gain, norm_rows) + exchange(out_gain, out_rows)
 
     def turn_gain(i):
@@ -380,10 +379,9 @@
 
     for l in range(n_layers):
         last = l + 1 == n_layers
-        following = None if last else in_proj[l + 1]
         groups_of_rows = [pl.ds(m * group, group) for m in range(groups)]
         if l == 0:
-            waiting = list(out_proj[0][1:])
+            waiting = list(out_proj[0][early:])
             for d in range(1, nz):
                 for k in range(stream_pieces):
                     spread.step(d, k, cross.forward)
@@ -399,66 +397,58 @@
                     @pl.when(spread.has[way, d])
                     def _():
                         spread.wait_hand(way, d)
-            for half, (parts, buf) in enumerate(zip(in_proj[l], (v_buf, g_buf))):
-                total = None
+        for half, (part, buf) in enumerate(zip(in_proj[l], (v_buf, g_buf))):
+            total = None
+            for k in range(ny):
+                part.arrive(k, 0)
+                slot = slot_of(k, 0)
+                one = jnp.dot(buf[l, slot], h_all[l, rows_at(slot, f_cols), :], preferred_element_type=F32)
+                total = one if total is None else total + one
+            acc[half] = total
+        for k in range(stream_pieces):
+            for way in (1, -1):
+                cross.receive(way, nz - 1, k)
+        cross.finish()
+        if l > 0:
+            for j in range(1, nx):
+                factor_copies[j - 1].wait_recv()
+                scale = peer_factor[l - 1, j - 1, 0:1, :]
                 for k in range(ny):
-                    for part in parts:
-                        part.arrive(k, 0)
-                    slot = slot_of(k, 0)
-                    one = jnp.dot(buf[l, slot], h_all[l, rows_at(slot, f_cols), :], preferred_element_type=F32)
-                    total = one if total is None else total + one
-                acc[half] = total
-            for k in range(stream_pieces):
-                for way in (1, -1):
-                    cross.receive(way, nz - 1, k)
-            cross.finish()
-            part_copies = {}
-            for m, rows in enumerate(groups_of_rows):
-                for j in range(1, nx):
-                    for half, buf in enumerate((v_buf, g_buf)):
-                        total = None
-                        for k in range(ny):
-                            block = rows_at(lax.rem(y + ny - k, ny), f_cols)
-                            one = jnp.dot(
-                                buf[l, slot_of(k, 0), rows, :], x_all[j - 1, block, :],
-                                preferred_element_type=F32,
-                            )
-                            total = one if total is None else total + one
-                        part_out[j - 1, half, rows, :] = total.astype(BF16)
-                    mine = part_out.at[j - 1, :, rows, :]
-                    send = send_slot()
-                    copy = remote(
-                        mine, part_in.at[j - 1, :, rows, :], y * nx + lax.rem(x + nx - j, nx), t,
-                        send, recv_slot(),
-                    )
-                    start(copy)
-                    leave(mine, send)
-                    part_copies[m, j] = copy
-            for part in out_proj[0]:
-                part.send_y()
-        else:
-            for part in in_proj[l][0] + in_proj[l][1]:
-                part.flush()
-            for k, j in steps:
-                slot = slot_of(k, j)
-                for half, (parts, buf) in enumerate(zip(in_proj[l], (v_buf, g_buf))):
-                    for part in parts:
-                        part.arrive(k, j)
-                    one = jnp.dot(buf[l, slot], h_all[l, rows_at(slot, f_cols), :], preferred_element_type=F32)
-                    if (k, j) == (0, 0):
-                        acc[half] = one
-                    else:
-                        acc[half] += one
+                    here = pl.ds(k * f_cols, f_cols)
+                    gain = out_cols[rows_at(k * nx + x, f_cols), l - 1 : l]
+                    change = x_branch[l - 1, j - 1, here, :].astype(F32) * scale * gain
+                    x_all[l, j - 1, here, :] = (x_all[l - 1, j - 1, here, :].astype(F32) + change).astype(BF16)
+        part_copies = {}
+        for m, rows in enumerate(groups_of_rows):
+            for j in range(1, nx):
+                for half, buf in enumerate((v_buf, g_buf)):
+                    total = None
+                    for k in range(ny):
+                        block = rows_at(lax.rem(y + ny - k, ny), f_cols)
+                        one = jnp.dot(
+                            buf[l, slot_of(k, 0), rows, :], x_all[l, j - 1, block, :],
+                            preferred_element_type=F32,
+                        )
+                        total = one if total is None else total + one
+                    part_out[l, j - 1, half, rows, :] = total.astype(BF16)
+                mine = part_out.at[l, j - 1, :, rows, :]
+                send = send_slot()
+                copy = remote(
+                    mine, part_in.at[l, j - 1, :, rows, :], y * nx + lax.rem(x + nx - j, nx), t,
+                    send, recv_slot(),
+                )
+                start(copy)
+                leave(mine, send)
+                part_copies[m, j] = copy
 
         edges = []
         for m, rows in enumerate(groups_of_rows):
             lanes = pl.ds(m * group, group)
             value, gate = acc[0, rows, :], acc[1, rows, :]
-            if l == 0:
-                for j in range(1, nx):
-                    part_copies[m, j].wait_recv()
-                    value = value + part_in[j - 1, 0, rows, :].astype(F32)
-                    gate = gate + part_in[j - 1, 1, rows, :].astype(F32)
+            for j in range(1, nx):
+                part_copies[m, j].wait_recv()
+                value = value + part_in[l, j - 1, 0, rows, :].astype(F32)
+                gate = gate + part_in[l, j - 1, 1, rows, :].astype(F32)
             gated = (value * jax.nn.sigmoid(gate)).astype(BF16)
             wide[l, pl.ds(EDGE, positions), lanes] = gated.astype(F32).T
             pair = []
@@ -473,14 +463,8 @@
             to_right, to_left = pair
             edges.append((to_right, to_left))
 
-        if l == 0:
-            if following is not None:
-                following[0][0].send_x()
-                for part in following[1] + following[0]:
-                    part.send_y()
-        if last:
-            for part in out_proj[l]:
-                part.send_x()
+        for part in out_proj[l][:early] if l == 0 else out_proj[l]:
+            part.flush()
 
         blank = jnp.zeros((EDGE, channels), F32)
 
@@ -560,7 +544,7 @@
         def activate_inner(block):
             activate(conv_all, block, EDGE, positions - 2 * EDGE, EDGE)
 
-        def drain(spread, ready, consume, hook, finish=None):
+        def drain(spread, ready, consume, hook, finish=None, extra=None):
             def take(d):
                 for way in (1, -1):
                     @pl.when(spread.has[way, d])
@@ -572,7 +556,7 @@
             when = min(2, nz - 1)
             for d in range(1, nz):
                 for k in range(spread.pieces):
-                    spread.step(d, k)
+                    spread.step(d, k, extra)
                     hook((d - 1) * spread.pieces + k)
                 if d == when:
                     ready()
@@ -594,16 +578,10 @@
                 if i >= 2 and turned[0] < n_tp:
                     turn_gain(turned[0])
                     turned[0] += 1
-                if i == 1:
-                    for part in out_proj[l][: out_parts // 2]:
-                        part.relay()
-                if i == 4:
-                    for part in out_proj[l][out_parts // 2 :]:
-                        part.relay()
-                if i == 5 and following is not None:
-                    following[0][1].send_x()
-            if last and i % 3 == 0 and 0 < i // 3 <= out_parts:
-                out_proj[l][i // 3 - 1].flush()
+                if i % 3 == 1 and early + i // 3 < out_parts:
+                    out_proj[l][early + i // 3].flush()
+            if not last and i == 5:
+                out_proj[l + 1][0].send_x()
 
         def catch_edges():
             for d in range(1, nz):
@@ -652,34 +630,41 @@
         else:
             branch_all[l, my_rows, :] = narrow_branch
             branch_spread = row_spread(branch_all.at[l])
+            cross = Cross(branch_spread, x_branch.at[l])
             for k in range(stream_pieces):
                 branch_spread.start_own(k)
-            if l == 0:
-                for part in following[0] + following[1]:
-                    part.send_x()
-
-            factor = [None]
-
-            def scale():
+                cross.forward(1, 0, k)
+            for part in out_proj[l + 1]:
+                part.send_y()
+
+            factor, factor_copies = [None], []
+
+            def scale_up():
                 factor[0] = factor_of()
+                own_factor[l, 0:1, :] = factor[0]
+                for j in range(1, nx):
+                    mine, send = own_factor.at[l], send_slot()
+                    copy = remote(mine, peer_factor.at[l, j - 1], x_peer(j), t, send, recv_slot())
+                    start(copy)
+                    leave(mine, send)
+                    factor_copies.append(copy)
 
             def renew(block):
-                rows = rows_at(block, features)
-                gain = out_cols[rows, l : l + 1]
-                change = branch_all[l, rows, :].astype(F32) * factor[0] * gain
-                h_all[l + 1, rows, :] = (h_all[l, rows, :].astype(F32) + change).astype(BF16)
+                @pl.when((block == t) | (lax.rem(block // 2, nx) == x))
+                def _():
+                    rows = rows_at(block, features)
+                    gain = out_cols[rows, l : l + 1]
+                    change = branch_all[l, rows, :].astype(F32) * own_factor[l, 0:1, :] * gain
+                    h_all[l + 1, rows, :] = (h_all[l, rows, :].astype(F32) + change).astype(BF16)
 
             def branch_hook(i):
-                if i == stream_pieces:
-                    following[1][0].relay()
-                    following[0][0].relay()
-                if i == stream_pieces + 2:
-                    following[1][1].relay()
-                    following[0][1].relay()
-                    for part in out_proj[l + 1]:
-                        part.send_y()
-
-            drain(branch_spread, scale, renew, branch_hook)
+                d, k = i // stream_pieces + 1, i % stream_pieces
+                for way in ((1,) if d == 1 else (1, -1)):
+                    cross.receive(way, d - 1, k)
+                if i % 2 == 1 and 1 + i // 2 < out_parts:
+                    out_proj[l + 1][1 + i // 2].send_x()
+
+            drain(branch_spread, scale_up, renew, branch_hook, extra=cross.forward)
 
     for copy, condition in sent:
         if condition is None:
@@ -694,11 +679,11 @@
 def slots_of(ny, nx, nz, layers, features, channels, positions):
     n_sp, far = ny * nx, 2 * (nz - 1)
     pieces, cuts, groups = pieces_of(features, 128), len(cuts_of(positions)), pieces_of(channels, LANES)
-    small = 2 + 3 * layers + groups * (nx - 1) + 2 * groups * layers
-    send = 3 * layers * (1 + 2 * far) + (far + 1) * nx + 3 * layers + small
-    recv = layers * (3 + far * (pieces + 1 + cuts + 1 + 2)) + (far + 1) * (pieces + 1) * (nx - 1)
-    recv += 2 * (ny - 1) + (n_sp - 1) * (4 * (layers - 1) + pieces * layers) + small
-    local = 1 + 2 + 4 * (layers - 1) + pieces * layers
+    small = 2 + 3 * layers + groups * (nx - 1) * layers + 2 * groups * layers + (layers - 1) * (nx - 1)
+    send = layers * (3 * (1 + 2 * far) + (far + 1) * nx + 3) + small
+    recv = layers * (3 + far * (pieces + 1 + cuts + 1 + 2) + (far + 1) * (pieces + 1) * (nx - 1)) + small
+    recv += layers * (2 * (ny - 1) + (n_sp - 1) * pieces)
+    local = 1 + layers * (2 + pieces)
     return send, recv, local
 
 
@@ -717,7 +702,10 @@
         out_specs=vmem,
         scratch_shapes=[
             pltpu.VMEM((layers, n_tp * features, positions), BF16),
-            pltpu.VMEM((nx - 1, n_tp * features // nx, positions), BF16),
+            pltpu.VMEM((layers, nx - 1, n_tp * features // nx, positions), BF16),
+            pltpu.VMEM((max(layers - 1, 1), nx - 1, n_tp * features // nx, positions), BF16),
+            pltpu.VMEM((layers, 1, positions), F32),
+            pltpu.VMEM((layers, nx - 1, 1, positions), F32),
             pltpu.VMEM((layers, n_tp, positions, channels), BF16),
             pltpu.VMEM((layers, n_tp, 2 * EDGE, channels), BF16),
             pltpu.VMEM((max(layers - 1, 1), n_tp * features, positions), BF16),
@@ -725,8 +713,8 @@
             pltpu.VMEM((layers, n_sp, channels, f_cols), BF16),
             pltpu.VMEM((layers, n_sp, channels, f_cols), BF16),
             pltpu.VMEM((layers, n_sp, features, c_cols), BF16),
-            pltpu.VMEM((nx - 1, 2, channels, positions), BF16),
-            pltpu.VMEM((nx - 1, 2, channels, positions), BF16),
+            pltpu.VMEM((layers, nx - 1, 2, channels, positions), BF16),
+            pltpu.VMEM((layers, nx - 1, 2, channels, positions), BF16),
             pltpu.VMEM((layers, positions + 2 * EDGE, channels), F32),
             pltpu.VMEM((2, positions, channels), F32),
             pltpu.VMEM((layers, 2 * EDGE, channels), F32),

time: 120 us -> 115 us (0.958)
  Pallas kernels: 117 us -> 113 us
    pallas_call x1, Pallas kernels: 117 us -> 113 us  [on_device(): pl.pallas_call(functools.partial(kernel, n_sp, n_tp, layers), out_shape=j...]
where the time goes in v3:
time: 115 us
  Pallas kernels  113 us (98%)
  local copies, waits for them, and re-layouts  1.67 us (1%)
    pallas_call x1, Pallas kernels, on_device(): pl.pallas_call(functools.partial(kernel, n_sp, n_tp, layers), out_shape=j...  113 us

profile of v3, /device:TPU:0, one launch (start us, length us, event | category | flops | bytes accessed | tf_op | source)
XLA Modules:
  0.0 114.7 jit_solution(1029833034975988092)
XLA Ops:
  0.0 113.0 %shard_map.73 = bf16[512,256]{1,0:T(8,128)(2,1)} custom-call(bf16[512,256]{1,0:T(8,128)(2,1)} %stream.1, bf16[2,256,1024]{2,1,0:T(8,128)(2,1)} %value_w.1, bf16[2,256,1024]{2,1,0:T(8,128)(2,1)} %gate_w.1, bf16[31,2,256]{2,1,0:T(2,128)(2,1)} %bitcast.1, bf16[2,256]{1,0:T(2,128)(2,1)} %norm_gain.1, bf16[2,512,512]{2,1,0:T(8,128)(2,1)} %out_w.1, ...), custom_call_target="tpu_custom_call" | custom-call | tf_op jit(solution)/shard_map/pallas_call | solution.py:698
  113.0 1.7 %copy.9 = bf16[512,256]{1,0:T(8,128)(2,1)} copy(bf16[512,256]{1,0:T(8,128)(2,1)} %shard_map.73) | data formatting | bytes 524288

commit v4 on v3

--- a/solution.py
+++ b/solution.py
@@ -82,8 +82,32 @@
         else:
             pl.when(condition)(copy.start)
 
+    tag, banks = [None], {}
+
     def leave(ref, send, condition=None):
-        sent.append((remote(ref, ref, s, t, send=send), condition))
+        sent.append((remote(ref, ref, s, t, send=send), condition, tag[0]))
+
+    def finish_sends(name=None):
+        chosen = [entry for entry in sent if name is None or entry[2] == name]
+        sent[:] = [entry for entry in sent if name is not None and entry[2] != name]
+        for entry in chosen:
+            if entry[1] is None:
+                entry[0].wait_send()
+            else:
+                pl.when(entry[1])(entry[0].wait_send)
+
+    def banked(name, make):
+        here, tag[0] = (sends[0], recvs[0]), name
+        again = name in banks
+        if again:
+            assert not [entry for entry in sent if entry[2] == name]
+            sends[0], recvs[0] = banks[name]
+        banks.setdefault(name, here)
+        made = make()
+        if again:
+            sends[0], recvs[0] = here
+        tag[0] = None
+        return made
 
     def slot_of(k, j):
         return lax.rem(y + ny - k, ny) * nx + lax.rem(x + nx - j, nx)
@@ -238,11 +262,28 @@
         def wait_hand(self, way, d):
             self.handed[way, d].wait_recv()
 
+    def ways_at(d):
+        return (1, -1) if d else (1,)
+
     class Cross:
         def __init__(self, spread, land):
             self.spread, self.land = spread, land
             self.size = features // spread.pieces
             self.sends, self.base, self.hands = {}, {}, {}
+            for d in range(nz):
+                for way in ways_at(d):
+                    ok, q, owner = self.facts(way, d)
+                    block = self.rows(q, 0, spread.pieces)
+                    self.sends[way, d] = send_slot()
+                    leave(land.at[0, block, :], self.sends[way, d], ok & (owner != x))
+                    for k in range(spread.pieces):
+                        self.base[way, d, k] = recv_slot(nx - 1)
+                    for j in range(1, nx):
+                        send, recv = send_slot(), recv_slot()
+                        place = land.at[j - 1, block, :]
+                        mine = ok & (owner == x)
+                        self.hands[way, d, j] = (send, recv, remote(place, place, s, t, recv=recv), mine)
+                        leave(place, send, mine)
 
         def facts(self, way, d):
             zz = z - way * d
@@ -258,30 +299,29 @@
         def forward(self, way, d, k):
             ok, q, owner = self.facts(way, d)
             pick = jnp.clip(lax.rem(owner - x + nx, nx) - 1, 0, nx - 2)
-            if (way, d) not in self.sends:
-                self.sends[way, d] = send_slot()
-                leave(self.land.at[0, self.rows(q, 0, self.spread.pieces), :], self.sends[way, d], ok & (owner != x))
-            base = self.base[way, d, k] = recv_slot(nx - 1)
             copy = remote(
                 self.spread.place(q, c, k), self.land.at[pick, self.rows(q, k), :], y * nx + owner, t,
-                self.sends[way, d], base + pick,
+                self.sends[way, d], self.base[way, d, k] + pick,
             )
             start(copy, ok & (owner != x))
 
         def receive(self, way, d, k):
-            ok, q, owner = self.facts(way, d)
-            mine = ok & (owner == x)
+            _, q, _ = self.facts(way, d)
             for j in range(1, nx):
-                if k == 0:
-                    block = self.land.at[j - 1, self.rows(q, 0, self.spread.pieces), :]
-                    send, recv = send_slot(), recv_slot()
-                    self.hands[way, d, j] = (send, recv, remote(block, block, s, t, recv=recv), mine)
-                    leave(block, send, mine)
-                send, recv, _, _ = self.hands[way, d, j]
+                send, recv, _, mine = self.hands[way, d, j]
                 here = self.land.at[j - 1, self.rows(q, k), :]
                 landed = remote(here, here, s, t, recv=self.base[way, d, k] + j - 1)
-                pl.when(mine)(landed.wait_recv)
-                start(remote(here, here, s, z * 2 + 1 - c, send, recv), mine)
+                hand = remote(here, here, s, z * 2 + 1 - c, send, recv)
+
+                @pl.when(mine)
+                def _():
+                    landed.wait_recv()
+                    hand.start()
+
+        def receive_all(self, d):
+            for k in range(self.spread.pieces):
+                for way in ways_at(d):
+                    self.receive(way, d, k)
 
         def finish(self):
             for _, _, handed, mine in self.hands.values():
@@ -325,14 +365,17 @@
 
     stream_copy = local_copy(stream, h_all.at[0, my_rows, :])
     barrier = pltpu.get_barrier_semaphore()
-    for k in range(1, n_sp):
-        pl.semaphore_signal(
-            barrier, inc=1, device_id={"sp": lax.rem(s + k, n_sp), "tp": t}, device_id_type=MESH
-        )
-    for k in range(1, n_tp):
-        pl.semaphore_signal(
-            barrier, inc=1, device_id={"sp": s, "tp": lax.rem(t + k, n_tp)}, device_id_type=MESH
-        )
+    above, below = z + 1 < nz, z > 0
+    near = [(x_peer(j), t, None) for j in range(1, nx)] + [(y_peer(k), t, None) for k in range(1, ny)]
+    near += [(s, z * 2 + 1 - c, None), (s, (z + 1) * 2 + c, above), (s, (z - 1) * 2 + c, below)]
+    for sp, tp, here in near:
+        def greet(sp=sp, tp=tp):
+            pl.semaphore_signal(barrier, inc=1, device_id={"sp": sp, "tp": tp}, device_id_type=MESH)
+
+        if here is None:
+            greet()
+        else:
+            pl.when(here)(greet)
     in_proj, out_proj = [], []
     out_parts = pieces_of(features, 128)
     for l in range(n_layers):
@@ -344,10 +387,16 @@
     for l in range(n_layers):
         tap_rows[l, 0:n_taps, :] = taps[:, l, :].astype(F32)
     stream_copy.wait()
-    pl.semaphore_wait(barrier, n_sp + n_tp - 2)
-
-    spread = row_spread(h_all.at[0])
-    cross = Cross(spread, x_all.at[0])
+    @pl.when(above & below)
+    def _():
+        pl.semaphore_wait(barrier, nx + ny + 1)
+
+    @pl.when(jnp.logical_not(above & below))
+    def _():
+        pl.semaphore_wait(barrier, nx + ny)
+
+    spread = banked("rows", lambda: row_spread(h_all.at[0]))
+    cross = banked("cross", lambda: Cross(spread, x_all.at[0]))
     for k in range(stream_pieces):
         spread.start_own(k)
         cross.forward(1, 0, k)
@@ -359,7 +408,6 @@
     for l in range(1, n_layers):
         for part in in_proj[l]:
             part.send_y()
-    gain_copies = exchange(norm_gain, norm_rows) + exchange(out_gain, out_rows)
 
     def turn_gain(i):
         rows = out_rows[i].astype(F32)
@@ -385,8 +433,8 @@
             for d in range(1, nz):
                 for k in range(stream_pieces):
                     spread.step(d, k, cross.forward)
-                    for way in ((1,) if d == 1 else (1, -1)):
-                        cross.receive(way, d - 1, k)
+                    for way in ways_at(d - 2) if d > 1 else ():
+                        cross.receive(way, d - 2, k)
                     if waiting and ((d - 1) * stream_pieces + k) % 2 == 1:
                         waiting.pop(0).send_x()
             for part in waiting:
@@ -397,6 +445,9 @@
                     @pl.when(spread.has[way, d])
                     def _():
                         spread.wait_hand(way, d)
+            gain_copies = exchange(norm_gain, norm_rows) + exchange(out_gain, out_rows)
+        if nz > 1:
+            cross.receive_all(nz - 2)
         for half, (part, buf) in enumerate(zip(in_proj[l], (v_buf, g_buf))):
             total = None
             for k in range(ny):
@@ -405,9 +456,7 @@
                 one = jnp.dot(buf[l, slot], h_all[l, rows_at(slot, f_cols), :], preferred_element_type=F32)
                 total = one if total is None else total + one
             acc[half] = total
-        for k in range(stream_pieces):
-            for way in (1, -1):
-                cross.receive(way, nz - 1, k)
+        cross.receive_all(nz - 1)
         cross.finish()
         if l > 0:
             for j in range(1, nx):
@@ -503,7 +552,7 @@
             sums[l, phase, t, 1:2, :] = (across_lanes(ones, high) + across_lanes(ones, low))[0:1]
             return exchange(sums.at[l, phase, t], sums.at[l, phase])
 
-        inner, edge = position_spreads(conv_all.at[l], conv_edge.at[l])
+        inner, edge = banked("conv", lambda: position_spreads(conv_all.at[l], conv_edge.at[l]))
         border = jnp.zeros((EDGE, channels), BF16)
         conv_all[l, t, 0:EDGE, :] = border
         conv_all[l, t, positions - EDGE : positions, :] = border
@@ -575,13 +624,16 @@
             if l == 0:
                 if i == 2:
                     arrived(gain_copies)
+                    finish_sends("rows")
+                    finish_sends("cross")
                 if i >= 2 and turned[0] < n_tp:
                     turn_gain(turned[0])
                     turned[0] += 1
                 if i % 3 == 1 and early + i // 3 < out_parts:
                     out_proj[l][early + i // 3].flush()
-            if not last and i == 5:
-                out_proj[l + 1][0].send_x()
+            if not last and i in (3, 5):
+                for part in out_proj[l + 1][: i // 2]:
+                    part.send_x()
 
         def catch_edges():
             for d in range(1, nz):
@@ -629,8 +681,8 @@
             result[...] = fresh.astype(BF16)
         else:
             branch_all[l, my_rows, :] = narrow_branch
-            branch_spread = row_spread(branch_all.at[l])
-            cross = Cross(branch_spread, x_branch.at[l])
+            branch_spread = banked("rows", lambda: row_spread(branch_all.at[l]))
+            cross = banked("cross", lambda: Cross(branch_spread, x_branch.at[l]))
             for k in range(stream_pieces):
                 branch_spread.start_own(k)
                 cross.forward(1, 0, k)
@@ -659,18 +711,16 @@
 
             def branch_hook(i):
                 d, k = i // stream_pieces + 1, i % stream_pieces
-                for way in ((1,) if d == 1 else (1, -1)):
-                    cross.receive(way, d - 1, k)
+                for way in ways_at(d - 2) if d > 1 else ():
+                    cross.receive(way, d - 2, k)
+                if i == 2:
+                    finish_sends("conv")
                 if i % 2 == 1 and 1 + i // 2 < out_parts:
                     out_proj[l + 1][1 + i // 2].send_x()
 
             drain(branch_spread, scale_up, renew, branch_hook, extra=cross.forward)
 
-    for copy, condition in sent:
-        if condition is None:
-            copy.wait_send()
-        else:
-            pl.when(condition)(copy.wait_send)
+    finish_sends()
     assert sends[0] == send_sem.shape[0], sends
     assert recvs[0] == recv_sem.shape[0], recvs
     assert local_count[0] == local_sem.shape[0], local_count
@@ -680,8 +730,8 @@
     n_sp, far = ny * nx, 2 * (nz - 1)
     pieces, cuts, groups = pieces_of(features, 128), len(cuts_of(positions)), pieces_of(channels, LANES)
     small = 2 + 3 * layers + groups * (nx - 1) * layers + 2 * groups * layers + (layers - 1) * (nx - 1)
-    send = layers * (3 * (1 + 2 * far) + (far + 1) * nx + 3) + small
-    recv = layers * (3 + far * (pieces + 1 + cuts + 1 + 2) + (far + 1) * (pieces + 1) * (nx - 1)) + small
+    send = 3 * (1 + 2 * far) + (far + 1) * nx + 3 * layers + small
+    recv = 3 + far * (pieces + 1 + cuts + 1 + 2) + (far + 1) * (pieces + 1) * (nx - 1) + small
     recv += layers * (2 * (ny - 1) + (n_sp - 1) * pieces)
     local = 1 + layers * (2 + pieces)
     return send, recv, local

time: 115 us -> 110 us (0.957)
  Pallas kernels: 113 us -> 108 us
    pallas_call x1, Pallas kernels: 113 us -> 108 us  [on_device(): pl.pallas_call(functools.partial(kernel, n_sp, n_tp, layers), out_shape=j...]
where the time goes in v4:
time: 110 us
  Pallas kernels  108 us (98%)
  local copies, waits for them, and re-layouts  1.67 us (2%)
    pallas_call x1, Pallas kernels, on_device(): pl.pallas_call(functools.partial(kernel, n_sp, n_tp, layers), out_shape=j...  108 us

profile of v4, /device:TPU:0, one launch (start us, length us, event | category | flops | bytes accessed | tf_op | source)
XLA Modules:
  0.0 110.1 jit_solution(11692499269870289587)
XLA Ops:
  0.0 108.4 %shard_map.73 = bf16[512,256]{1,0:T(8,128)(2,1)} custom-call(bf16[512,256]{1,0:T(8,128)(2,1)} %stream.1, bf16[2,256,1024]{2,1,0:T(8,128)(2,1)} %value_w.1, bf16[2,256,1024]{2,1,0:T(8,128)(2,1)} %gate_w.1, bf16[31,2,256]{2,1,0:T(2,128)(2,1)} %bitcast.1, bf16[2,256]{1,0:T(2,128)(2,1)} %norm_gain.1, bf16[2,512,512]{2,1,0:T(8,128)(2,1)} %out_w.1, ...), custom_call_target="tpu_custom_call" | custom-call | tf_op jit(solution)/shard_map/pallas_call | solution.py:748
  108.4 1.7 %copy.9 = bf16[512,256]{1,0:T(8,128)(2,1)} copy(bf16[512,256]{1,0:T(8,128)(2,1)} %shard_map.73) | data formatting | bytes 524288

commit v5 on v4

--- a/solution.py
+++ b/solution.py
@@ -629,8 +629,8 @@
                 if i >= 2 and turned[0] < n_tp:
                     turn_gain(turned[0])
                     turned[0] += 1
-                if i % 3 == 1 and early + i // 3 < out_parts:
-                    out_proj[l][early + i // 3].flush()
+                if i in (1, 3) and early + i // 2 < out_parts:
+                    out_proj[l][early + i // 2].flush()
             if not last and i in (3, 5):
                 for part in out_proj[l + 1][: i // 2]:
                     part.send_x()

time: 110 us -> 108 us (0.982)
  Pallas kernels: 108 us -> 106 us
    pallas_call x1, Pallas kernels: 108 us -> 106 us  [on_device(): pl.pallas_call(functools.partial(kernel, n_sp, n_tp, layers), out_shape=j...]
where the time goes in v5:
time: 108 us
  Pallas kernels  106 us (98%)
  local copies, waits for them, and re-layouts  1.67 us (2%)
    pallas_call x1, Pallas kernels, on_device(): pl.pallas_call(functools.partial(kernel, n_sp, n_tp, layers), out_shape=j...  106 us

profile of v5, /device:TPU:0, one launch (start us, length us, event | category | flops | bytes accessed | tf_op | source)
XLA Modules:
  0.0 107.8 jit_solution(12765041114315420483)
XLA Ops:
  0.0 106.1 %shard_map.73 = bf16[512,256]{1,0:T(8,128)(2,1)} custom-call(bf16[512,256]{1,0:T(8,128)(2,1)} %stream.1, bf16[2,256,1024]{2,1,0:T(8,128)(2,1)} %value_w.1, bf16[2,256,1024]{2,1,0:T(8,128)(2,1)} %gate_w.1, bf16[31,2,256]{2,1,0:T(2,128)(2,1)} %bitcast.1, bf16[2,256]{1,0:T(2,128)(2,1)} %norm_gain.1, bf16[2,512,512]{2,1,0:T(8,128)(2,1)} %out_w.1, ...), custom_call_target="tpu_custom_call" | custom-call | tf_op jit(solution)/shard_map/pallas_call | solution.py:748
  106.1 1.7 %copy.9 = bf16[512,256]{1,0:T(8,128)(2,1)} copy(bf16[512,256]{1,0:T(8,128)(2,1)} %shard_map.73) | data formatting | bytes 524288
